TPU v7x, 512 devices: a whole 4x4x16 slice. The times are simulated.
512 devices in a mesh: kv: 64 (over z, y), tp: 8 (over x, core).
Axes of the slice: x: 4, y: 4, z: 16, core: 2. Of those that a mesh axis runs over, the one named last changes fastest.
Arguments:
- queries: bfloat16 [57344, 1024], P('kv', 'tp'), may hold values from -6 to 6
- keyvals: bfloat16 [57344, 128], P('kv'), may hold values from -6 to 6
- log_sums: float32 [16, 57344], P('tp', 'kv'), may hold values from 6 to 7.2
- out_grad: bfloat16 [57344, 1024], P('kv', 'tp'), may hold values from -24 to 24
- inputs: bfloat16 [57344, 2048], P('kv'), may hold values from -0.3125 to 0.3125
- selection: int32 [448, 16], replicated, may hold values from -1 to 1791, as said below
Outputs:
- query_grad: bfloat16 [57344, 1024], P('kv', 'tp')
- keyval_grad: float32 [1792, 32, 128], P('kv', 'tp')
- weight_grad: float32 [2048, 1024], P('kv', 'tp')
Inputs may be any that keep to these rules, and one draw needn't show every extreme that they name: `selection`: row j first names the key blocks of query block j's own positions in order, then distinct blocks of earlier devices' positions, then -1 entries at the end (only where fewer earlier blocks exist). The rows of one device's query blocks together name at most 2 distinct blocks of any one other device, and exactly 2 for some pair in every draw.
All inputs are finite; a program needn't handle non-finite values.
Results may differ from a plain program's by a relative error of at most 0.0071.
Values may be sent and summed in bfloat16 or wider, within the bound.
No kernel may reach another device: no remote copies, remote signals or barrier semaphores. Data moves between devices by JAX's collectives and lax.ppermute only.
A program may use at most 64 MiB of HBM per device.

v0:
```python
import jax
import jax.numpy as jnp
from jax import lax
from jax.experimental import pallas as pl
from jax.experimental.pallas import tpu as pltpu
from jax.sharding import Mesh
from jax.sharding import PartitionSpec as P

DH = 64
QB = 128
KB = 32
NSEL = 16
CAP = 2

TOK = 896
PER = TOK // QB
OWN = TOK // KB
KV = 64
TP = 8
DIAG = QB // KB
REM = NSEL - DIAG
PIECE = KB // TP
ROWS = NSEL * PIECE
REM_ROWS = REM * PIECE
KEYS = NSEL * KB
SLOTS = KV * CAP * PIECE
NONE = -4096
G_AT = QB
LOG_AT = 2 * QB
SEND = LOG_AT + 16
SLOT_ROWS = CAP * PIECE
W_ROWS = 32
NEAR, FAR = 4, 16
LOG2E = 1.4426950408889634

VMEM = pl.BlockSpec(memory_space=pltpu.VMEM)
HBM = pl.BlockSpec(memory_space=pltpu.HBM)
GRANT = 12 << 20
WEIGHT_GRANT = 56_000_000
ALL_VMEM = 67_040_000


def call(kernel, out_shape, args, scratch=(), specs=None, out_specs=None, grant=GRANT):
    return pl.pallas_call(
        kernel,
        out_shape=out_shape,
        in_specs=specs or [VMEM for _ in args],
        out_specs=out_specs or jax.tree.map(lambda _: VMEM, out_shape),
        scratch_shapes=list(scratch),
        compiler_params=pltpu.CompilerParams(vmem_limit_bytes=grant),
    )(*args)


def kv_index():
    return lax.axis_index("z") * NEAR + lax.axis_index("y")


def member_index():
    return lax.axis_index("x") * 2 + lax.axis_index("core")


def slot_blocks(pair_ref):
    second = lax.broadcasted_iota(jnp.int32, (SLOT_ROWS, 128), 0) >= PIECE
    rows = [
        jnp.where(
            second,
            jnp.broadcast_to(pair_ref[KV + d : KV + d + 1], (SLOT_ROWS, 128)),
            jnp.broadcast_to(pair_ref[d : d + 1], (SLOT_ROWS, 128)),
        )
        for d in range(KV)
    ]
    return jnp.concatenate(rows, axis=0)


def offer_kernel(
    sel_hbm, kv_hbm, q_hbm, g_hbm, log_hbm, out_ref, pair_ref, same_hbm, other_hbm, sel_ref, kv_ref, log_ref, term_ref, sems, own_sems
):
    get_sel = pltpu.make_async_copy(sel_hbm, sel_ref, sems.at[0])
    get_kv = pltpu.make_async_copy(kv_hbm, kv_ref, sems.at[1])
    get_log = pltpu.make_async_copy(log_hbm, log_ref, sems.at[2])
    get_sel.start()
    get_kv.start()
    get_log.start()
    x, core = lax.axis_index("x"), lax.axis_index("core")
    places = []
    for k in range(4):
        for to, side in ((same_hbm, core), (other_hbm, 1 - core)):
            block = ((x + k) & 3) * 2 + side
            places.append((to.at[k], pl.multiple_of(jnp.minimum(block, PER - 1) * QB, QB)))
    copies = []
    for j, (to, at) in enumerate(places):
        copies.append(pltpu.make_async_copy(q_hbm.at[pl.ds(at, QB)], to.at[pl.ds(0, QB)], own_sems.at[j, 0]))
        copies.append(pltpu.make_async_copy(g_hbm.at[pl.ds(at, QB)], to.at[pl.ds(G_AT, QB)], own_sems.at[j, 1]))
    for copy in copies:
        copy.start()
    me, member = kv_index(), member_index()
    row = lax.broadcasted_iota(jnp.int32, (128, TOK), 0)
    col = lax.broadcasted_iota(jnp.int32, (128, TOK), 1)
    mine = (row >> 2) * KB + member * PIECE + (row & (PIECE - 1)) == col
    mine = mine.astype(jnp.bfloat16)
    get_sel.wait()
    local = (sel_ref[...] - me * OWN).astype(jnp.float32)
    inside = (local >= 0) & (local < OWN)
    least = jnp.min(jnp.where(inside, local, 1000.0), axis=0, keepdims=True)
    most = jnp.max(jnp.where(inside, local, -1000.0), axis=0, keepdims=True)
    shape = (KV, KV * PER)
    lane = lax.broadcasted_iota(jnp.int32, shape, 1)
    first_lane = lax.broadcasted_iota(jnp.int32, shape, 0) * PER
    in_row = (lane >= first_lane) & (lane < first_lane + PER)
    least = jnp.min(jnp.where(in_row, least, 1000.0), axis=1, keepdims=True)
    most = jnp.max(jnp.where(in_row, most, -1000.0), axis=1, keepdims=True)
    other = lax.broadcasted_iota(jnp.int32, (KV, 128), 0) != me
    pair_ref[:KV] = jnp.where(other & (least < OWN), least, -1000.0)
    pair_ref[KV:] = jnp.where(other, most, -1000.0)
    get_log.wait()
    for j, (to, at) in enumerate(places):
        rest = log_ref[:, pl.ds(at, QB)]
        terms = []
        for _ in range(3):
            term = rest.astype(jnp.bfloat16).astype(jnp.float32)
            terms.append(term)
            rest = rest - term
        terms.append(jnp.zeros((10, QB), jnp.float32))
        term_ref[j] = jnp.concatenate(terms, axis=0).astype(jnp.bfloat16)
        copies.append(pltpu.make_async_copy(term_ref.at[j], to.at[pl.ds(LOG_AT, 16)], own_sems.at[j, 2]))
        copies[-1].start()
    get_kv.wait()
    piece = jnp.dot(mine, kv_ref[...], preferred_element_type=jnp.float32).astype(jnp.bfloat16)
    at = lax.broadcasted_iota(jnp.int32, (SLOT_ROWS, 128), 1) - (
        lax.broadcasted_iota(jnp.int32, (SLOT_ROWS, 128), 0) & (PIECE - 1)
    )
    at = jnp.where((at & (PIECE - 1)) == 0, at >> 2, -1).astype(jnp.float32)
    onehot = slot_blocks(pair_ref).reshape(KV, SLOT_ROWS, 128) == at[None]
    onehot = onehot.reshape(SLOTS, 128).astype(jnp.bfloat16)
    out_ref[...] = jnp.dot(onehot, piece, preferred_element_type=jnp.float32).astype(jnp.bfloat16)
    for copy in copies:
        copy.wait()


def slot_kernel(after_ref, pair_ref, slot_ref):
    piece_row = lax.broadcasted_iota(jnp.int32, (SLOTS, 128), 0) & (PIECE - 1)
    home = slot_blocks(pair_ref) * PIECE + piece_row.astype(jnp.float32)
    slot_ref[...] = home.T[:8]


def pick_kernel(target_ref, fetched_ref, out_ref):
    column = jnp.broadcast_to(target_ref[...], (128, KEYS)).T
    parts = [
        (column == lax.broadcasted_iota(jnp.int32, (KEYS, 128), 1).astype(jnp.float32) + 128.0 * j)
        for j in range(SLOTS // 128)
    ]
    onehot = jnp.concatenate([p.astype(jnp.bfloat16) for p in parts], axis=1)
    rows = jnp.dot(onehot, fetched_ref[...], preferred_element_type=jnp.float32).astype(jnp.bfloat16)
    for t in range(TP):
        out_ref[t] = rows[t * ROWS : t * ROWS + REM_ROWS]


def attention_kernel(
    bias_ref, own_ref, remote_ref, zero_ref, one_ref, two_ref, three_ref, out_ref,
    kv_ref, in_ref, sum_ref, mask_ref, *pair_refs
):
    score_refs, dprob_refs, left_refs = pair_refs[:2], pair_refs[2:4], pair_refs[4:]
    scale = DH ** (-0.5)
    x, core = lax.axis_index("x"), lax.axis_index("core")
    for p in range(TP):
        kv_ref[p * ROWS : p * ROWS + REM_ROWS] = remote_ref[p]
        kv_ref[p * ROWS + REM_ROWS : (p + 1) * ROWS] = own_ref[p]
    for k, ref in enumerate((zero_ref, one_ref, two_ref, three_ref)):
        in_ref[2 * k] = ref[0]
        in_ref[2 * k + 1] = ref[1]
    shape = (KEYS, QB)
    key = lax.broadcasted_iota(jnp.int32, shape, 0)
    query = lax.broadcasted_iota(jnp.int32, shape, 1)
    within = key & (ROWS - 1)
    position = ((within >> 2) - REM) * KB + (key >> 6) * PIECE + (within & (PIECE - 1))
    live = (within < REM_ROWS) | (position <= query)
    bias = jnp.broadcast_to(bias_ref[...], (QB, KEYS)).T
    mask_ref[...] = jnp.where(live, bias, -1e30)
    kv = kv_ref[...]
    key_t = kv[:, :DH].T
    keys = kv[:, :DH]
    values = kv[:, DH:]
    zero = jnp.zeros((2 * QB, DH), jnp.bfloat16)

    def side_by_side(i, begin):
        both = in_ref[i, begin : begin + QB]
        return jnp.concatenate([both[:, :DH], both[:, DH:]], axis=0)

    def begin(i):
        contract = (((1,), (1,)), ((), ()))
        score_refs[i % 2][...] = lax.dot_general(
            keys, side_by_side(i, 0), contract, preferred_element_type=jnp.float32
        )
        dprob_refs[i % 2][...] = lax.dot_general(
            values, side_by_side(i, G_AT), contract, preferred_element_type=jnp.float32
        )

    def middle(i):
        score_ref, dprob_ref = score_refs[i % 2], dprob_refs[i % 2]
        left_ref = left_refs[i % 2]
        terms = in_ref[i, LOG_AT:].astype(jnp.float32)
        logs = ((terms[0:2] + terms[2:4]) + terms[4:6]) * LOG2E
        step = 64
        for h in range(2):
            half = slice(h * QB, (h + 1) * QB)
            log = jnp.broadcast_to(logs[h : h + 1], (step, QB))
            delta = jnp.zeros((8, QB), jnp.float32)
            for c in range(0, KEYS, step):
                rows = slice(c, c + step)
                prob = jnp.exp2(score_ref[rows, half] * (scale * LOG2E) + (mask_ref[rows] - log))
                prob_b = prob.astype(jnp.bfloat16)
                left_ref[rows, 2 * QB + h * QB : 2 * QB + (h + 1) * QB] = prob_b
                score_ref[rows, half] = prob
                part = prob_b.astype(jnp.float32) * dprob_ref[rows, half]
                delta = delta + jnp.sum(part.reshape(step // 8, 8, QB), axis=0)
            delta = jnp.broadcast_to(jnp.sum(delta, axis=0, keepdims=True), (step, QB))
            for c in range(0, KEYS, step):
                rows = slice(c, c + step)
                left_ref[rows, half] = (score_ref[rows, half] * (dprob_ref[rows, half] - delta)).astype(jnp.bfloat16)

    def finish(i):
        left_ref = left_refs[i % 2]
        turned = jnp.dot(key_t, left_ref[:, : 2 * QB], preferred_element_type=jnp.float32) * scale
        right = jnp.concatenate(
            [
                jnp.concatenate([side_by_side(i, 0), zero], axis=1),
                jnp.concatenate([zero, side_by_side(i, G_AT)], axis=1),
            ],
            axis=0,
        )
        term = jnp.dot(left_ref[...], right, preferred_element_type=jnp.float32)
        sum_ref[...] = term if i == 0 else sum_ref[...] + term
        both = jnp.concatenate([turned[:, :QB], turned[:, QB:]], axis=0)
        giver = ((x - (i >> 1)) & 3) * 2 + (core ^ (i & 1))
        out_ref[giver, :QB] = both.T.astype(jnp.bfloat16)

    begin(0)
    for i in range(TP):
        if i + 1 < TP:
            begin(i + 1)
        middle(i)
        finish(i)
    lane = lax.broadcasted_iota(jnp.int32, (KEYS, 2 * DH), 1)
    total = sum_ref[...] * jnp.where(lane < DH, scale, 1.0)
    out_ref[:, QB:] = total.astype(jnp.bfloat16).reshape(TP, ROWS, 2 * DH)


CHUNK = 256


def weight_kernel(target_ref, grad_ref, in_hbm, out_ref, in_ref, turned_ref, sum_ref, sems):
    copies = []
    for t in range(PER):
        rows = pl.ds(t * QB, QB)
        copies.append(pltpu.make_async_copy(in_hbm.at[rows], in_ref.at[rows], sems.at[t]))
        copies[-1].start()
    row = lax.broadcasted_iota(jnp.int32, (SLOTS, KEYS), 0).astype(jnp.float32)
    onehot = (row == target_ref[...]).astype(jnp.bfloat16)
    entries = jnp.concatenate([grad_ref[t, QB:] for t in range(TP)], axis=0)
    spread = jnp.dot(onehot, entries, preferred_element_type=jnp.float32).astype(jnp.bfloat16)
    for z in range(FAR):
        for d in range(NEAR):
            at = (z * NEAR + d) * SLOT_ROWS
            out_ref[d, z, W_ROWS:] = spread[at : at + SLOT_ROWS]
    for t in range(PER):
        turned_ref[:, t * QB : (t + 1) * QB] = grad_ref[t, :QB].T
    begin = 0
    for end in (2, 4, 6, 7):
        for t in range(begin, end):
            copies[t].wait()
        left = turned_ref[:, begin * QB : end * QB]
        for i in range(in_ref.shape[1] // CHUNK):
            columns = pl.ds(i * CHUNK, CHUNK)
            term = jnp.dot(left, in_ref[begin * QB : end * QB, columns], preferred_element_type=jnp.float32)
            if begin > 0:
                term = term + sum_ref[:, columns]
            if end < PER:
                sum_ref[:, columns] = term
                continue
            term = term.T.astype(jnp.bfloat16)
            for half in range(2):
                for d in range(NEAR):
                    at = half * 128 + d * W_ROWS
                    out_ref[d, 2 * i + half, :W_ROWS] = term[at : at + W_ROWS]
        begin = end


def weight_term(target, grads, inputs):
    return call(
        weight_kernel,
        jax.ShapeDtypeStruct((NEAR, FAR, W_ROWS + SLOT_ROWS, 2 * DH), jnp.bfloat16),
        [target, grads, inputs],
        scratch=[
            pltpu.VMEM(inputs.shape, jnp.bfloat16),
            pltpu.VMEM((2 * DH, TOK), jnp.bfloat16),
            pltpu.VMEM((2 * DH, inputs.shape[1]), jnp.float32),
            pltpu.SemaphoreType.DMA((PER,)),
        ],
        specs=[VMEM, VMEM, HBM],
        grant=WEIGHT_GRANT,
    )


def regroup_kernel(in_ref, out_ref):
    for z in range(FAR):
        term = in_ref[0, z, :W_ROWS].astype(jnp.float32)
        for d in range(1, NEAR):
            term = term + in_ref[d, z, :W_ROWS].astype(jnp.float32)
        out_ref[z, :W_ROWS] = term.astype(jnp.bfloat16)
        for d in range(NEAR):
            at = W_ROWS + d * SLOT_ROWS
            out_ref[z, at : at + SLOT_ROWS] = in_ref[d, z, W_ROWS:]


def home_kernel(slot_ref, returned_ref, grads_ref, kv_grad_ref, weight_ref):
    term = returned_ref[0, :W_ROWS].astype(jnp.float32)
    for z in range(1, FAR):
        term = term + returned_ref[z, :W_ROWS].astype(jnp.float32)
    weight_ref[...] = term
    row = lax.broadcasted_iota(jnp.int32, (OWN * PIECE, SLOTS), 0).astype(jnp.float32)
    onehot = (row == slot_ref[0:1]).astype(jnp.bfloat16)
    slots = jnp.concatenate([returned_ref[z, W_ROWS:] for z in range(FAR)], axis=0)
    total = jnp.dot(onehot, slots, preferred_element_type=jnp.float32)
    own = [grads_ref[t, QB + REM_ROWS :, :].astype(jnp.float32) for t in range(PER)]
    kv_grad_ref[...] = total + jnp.concatenate(own, axis=0)


def swap(array, axis):
    return lax.all_to_all(array, axis, 0, 0, tiled=True)


def body(queries, keyvals, log_sums, out_grad, inputs, selection):
    kv_axes, tp_axes = ("z", "y"), ("x", "core")
    me = kv_index()
    member = member_index()
    bf16 = jnp.bfloat16

    part = jax.ShapeDtypeStruct((4, SEND, 2 * DH), bf16)
    offer, pairs, same, other = call(
        offer_kernel,
        [jax.ShapeDtypeStruct((SLOTS, 2 * DH), bf16), jax.ShapeDtypeStruct((2 * KV, 128), jnp.float32), part, part],
        [selection.T, keyvals, queries, out_grad, log_sums],
        scratch=[
            pltpu.VMEM((NSEL, KV * PER), jnp.int32),
            pltpu.VMEM((TOK, 2 * DH), bf16),
            pltpu.VMEM((2, TOK), jnp.float32),
            pltpu.VMEM((TP, 16, QB), bf16),
            pltpu.SemaphoreType.DMA((3,)),
            pltpu.SemaphoreType.DMA((TP, 3)),
        ],
        specs=[HBM] * 5,
        out_specs=[VMEM, VMEM, HBM, HBM],
        grant=ALL_VMEM,
    )
    fetched = swap(offer.reshape(KV, SLOT_ROWS, 2 * DH), kv_axes)

    other = lax.ppermute(other, "core", [(0, 1), (1, 0)])

    def shift(array, k):
        return lax.ppermute(array, "x", [(i, (i + k) % 4) for i in range(4)])

    blocks = [jnp.stack([same[k], other[k]]) for k in range(4)]
    two, one = shift(blocks[2], 2), shift(blocks[1], 1)

    mine = lax.dynamic_slice(selection, (me * PER, 0), (PER, NSEL))[:, DIAG:]
    flat = mine.reshape(-1)
    owner = flat // OWN
    alike = owner[:, None] == owner[None, :]
    least = jnp.min(jnp.where(alike, flat[None, :], 1 << 20), axis=1)
    slot = jnp.where(flat != least, PIECE, 0)
    target = jnp.where(flat >= 0, owner * SLOT_ROWS + slot, NONE).reshape(PER, REM)
    target = jnp.pad(target, ((0, 1), (0, DIAG)), constant_values=NONE)
    live = (target >= 0) | (
        (jnp.arange(NSEL)[None, :] >= REM) & (jnp.arange(TP)[:, None] < PER)
    )
    target = (target[:, :, None] + jnp.arange(PIECE)).reshape(1, KEYS).astype(jnp.float32)
    live = lax.dynamic_index_in_dim(live, member, 0, keepdims=True)
    bias = jnp.where(live, 0.0, -1e30).astype(jnp.float32)
    bias = jnp.broadcast_to(bias[:, None, :, None], (1, TP, NSEL, PIECE)).reshape(1, KEYS)
    own_at = jnp.minimum(member, PER - 1) * QB
    own = lax.dynamic_slice(keyvals, (own_at, 0), (QB, 2 * DH))
    own = own.reshape(DIAG, TP, PIECE, 2 * DH).transpose(1, 0, 2, 3).reshape(TP, DIAG * PIECE, 2 * DH)

    picked = call(
        pick_kernel, jax.ShapeDtypeStruct((TP, REM_ROWS, 2 * DH), bf16), [target, fetched.reshape(SLOTS, 2 * DH)]
    )
    remote = swap(picked, tp_axes)
    three = shift(blocks[3], 3)
    grads = call(
        attention_kernel,
        jax.ShapeDtypeStruct((TP, QB + ROWS, 2 * DH), bf16),
        [bias, own, remote, blocks[0], one, two, three],
        scratch=[
            pltpu.VMEM((KEYS, 2 * DH), bf16),
            pltpu.VMEM((TP, SEND, 2 * DH), bf16),
            pltpu.VMEM((KEYS, 2 * DH), jnp.float32),
            pltpu.VMEM((KEYS, QB), jnp.float32),
            *[pltpu.VMEM((KEYS, 2 * QB), jnp.float32)] * 4,
            *[pltpu.VMEM((KEYS, 4 * QB), bf16)] * 2,
        ],
    )
    grads = swap(grads, tp_axes)
    query_grad = grads[:PER, :QB].reshape(TOK, 2 * DH)
    near = swap(weight_term(target, grads, inputs), "y")
    far = call(regroup_kernel, jax.ShapeDtypeStruct((FAR, W_ROWS + NEAR * SLOT_ROWS, 2 * DH), bf16), [near])
    slots = call(
        slot_kernel,
        jax.ShapeDtypeStruct((8, SLOTS), jnp.float32),
        [far, pairs],
        specs=[pl.BlockSpec(memory_space=pl.ANY), VMEM],
    )
    far = swap(far, "z")
    keyval_grad, weight_grad = call(
        home_kernel,
        [
            jax.ShapeDtypeStruct((OWN * PIECE, 2 * DH), jnp.float32),
            jax.ShapeDtypeStruct((W_ROWS, 2 * DH), jnp.float32),
        ],
        [slots, far, grads],
    )
    return query_grad, keyval_grad.reshape(OWN, PIECE, 2 * DH), weight_grad


def solution(mesh):
    split = Mesh(mesh.devices.reshape(FAR, NEAR, 4, 2), ("z", "y", "x", "core"))
    kv, tp = ("z", "y"), ("x", "core")
    return jax.shard_map(
        body,
        mesh=split,
        in_specs=(P(kv, tp), P(kv, None), P(tp, kv), P(kv, tp), P(kv, None), P()),
        out_specs=(P(kv, tp), P(kv, tp, None), P(kv, tp)),
        check_vma=False,
    )
```

profile of v0, /device:TPU:32, one launch (start us, length us, event | category | flops | bytes accessed | tf_op | source)
XLA Modules:
  0.0 128.7 jit_solution(6459620334393446848)
XLA Ops:
  0.6 17.9 %shard_map.85 = (bf16[512,128]{1,0:T(8,128)(2,1)}, f32[128,128]{1,0:T(8,128)}, bf16[4,272,128]{2,1,0:T(8,128)(2,1)}, bf16[4,272,128]{2,1,0:T(8,128)(2,1)}) custom-call(s32[16,448]{1,0:T(8,128)} %bitcast.16, bf16[896,128]{1,0:T(8,128)(2,1)} %kv_hbm.1, bf16[896,128]{1,0:T(8,128)(2,1)} %q_hbm.1, bf16[896,128]{1,0:T(8,128)(2,1)} %g_hbm.1, f32[2,896]{1,0:T(2,128)} %log_hbm.1), custom_call_target="tpu_custom_call" | custom-call | tf_op jit(solution)/shard_map/pallas_call | solution.py:44
  18.6 18.4 %all-to-all-start = ((bf16[64,8,128]{2,1,0:T(8,128)(2,1)}), bf16[64,8,128]{2,1,0:T(8,128)(2,1)S(1)}, u32[]{:S(2)}, u32[]{:S(2)}) async-start(bf16[64,8,128]{2,1,0:T(8,128)(2,1)} %bitcast.14), calls=%async_computation | async-start | bytes 262144 | tf_op jit(solution)/shard_map/all_to_all | solution.py:329
  37.0 1.9 %collective-permute-start = (bf16[4,272,128]{2,1,0:T(8,128)(2,1)}, bf16[4,272,128]{2,1,0:T(8,128)(2,1)S(1)}, u32[]{:S(2)}, u32[]{:S(2)}) collective-permute-start(bf16[4,272,128]{2,1,0:T(8,128)(2,1)} %get-tuple-element.11), channel_id=1, source_target_pairs={{0,1},{1,0},{2,3},{3,2},{4,5},{5,4},{6,7},{7,6},{8,9},{9,8},{10,11... | collective-permute-start | bytes 835592 | tf_op jit(solution)/shard_map/ppermute | solution.py:357
  38.9 0.8 dynamic-slice
  39.9 0.2 select_reduce_fusion
  40.4 0.8 constant_dynamic-slice_fusion
  41.2 1.0 fusion.5
  42.2 4.9 %collective-permute-start.2 = (bf16[2,272,128]{2,1,0:T(8,128)(2,1)S(1)}, bf16[2,272,128]{2,1,0:T(8,128)(2,1)S(1)}, u32[]{:S(2)}, u32[]{:S(2)}) collective-permute-start(bf16[2,272,128]{2,1,0:T(8,128)(2,1)S(1)} %pad_maximum_fusion.2), channel_id=1, source_target_pairs={{0,4},{2,6},{4,0},{6,2},{1,5},{3,7},{5,1},{7,3},{8,12},{10,14},{12... | collective-permute-start | bytes 417800 | tf_op jit(solution)/shard_map/ppermute | solution.py:360
  47.2 3.0 %collective-permute-start.3 = (bf16[2,272,128]{2,1,0:T(8,128)(2,1)S(1)}, bf16[2,272,128]{2,1,0:T(8,128)(2,1)S(1)}, u32[]{:S(2)}, u32[]{:S(2)}) collective-permute-start(bf16[2,272,128]{2,1,0:T(8,128)(2,1)S(1)} %pad_maximum_fusion.3), channel_id=1, source_target_pairs={{0,6},{2,0},{4,2},{6,4},{1,7},{3,1},{5,3},{7,5},{8,14},{10,8},{12,... | collective-permute-start | bytes 417800 | tf_op jit(solution)/shard_map/ppermute | solution.py:360
  50.3 2.8 %collective-permute-start.1 = (bf16[2,272,128]{2,1,0:T(8,128)(2,1)S(1)}, bf16[2,272,128]{2,1,0:T(8,128)(2,1)S(1)}, u32[]{:S(2)}, u32[]{:S(2)}) collective-permute-start(bf16[2,272,128]{2,1,0:T(8,128)(2,1)S(1)} %pad_maximum_fusion.1), channel_id=1, source_target_pairs={{0,2},{2,4},{4,6},{6,0},{1,3},{3,5},{5,7},{7,1},{8,10},{10,12},{12... | collective-permute-start | bytes 417800 | tf_op jit(solution)/shard_map/ppermute | solution.py:360
  53.3 0.1 convert_element_type.6.target_ref
  53.4 0.3 all-to-all-done
  53.7 1.0 shard_map.86
  54.7 4.3 %all-to-all-start.1 = ((bf16[8,48,128]{2,1,0:T(8,128)(2,1)}), bf16[8,48,128]{2,1,0:T(8,128)(2,1)S(1)}, u32[]{:S(2)}, u32[]{:S(2)}) async-start(bf16[8,48,128]{2,1,0:T(8,128)(2,1)} %shard_map.86), calls=%async_computation.1 | async-start | bytes 196608 | tf_op jit(solution)/shard_map/all_to_all | solution.py:329
  59.0 5.7 %all-to-all-done.1.remote_ref = bf16[8,48,128]{2,1,0:T(8,128)(2,1)S(1)} async-done(((bf16[8,48,128]{2,1,0:T(8,128)(2,1)}), bf16[8,48,128]{2,1,0:T(8,128)(2,1)S(1)}, u32[]{:S(2)}, u32[]{:S(2)}) %all-to-all-start.1) | async-done | bytes 98336 | tf_op jit(solution)/shard_map/all_to_all | solution.py:329
  64.8 3.6 %shard_map.87 = bf16[8,192,128]{2,1,0:T(8,128)(2,1)S(1)} custom-call(f32[1,512]{1,0:T(1,128)S(1)} %broadcast_in_dim.54.bias_ref, bf16[8,16,128]{2,1,0:T(8,128)(2,1)S(1)} %bitcast.12, bf16[8,48,128]{2,1,0:T(8,128)(2,1)S(1)} %all-to-all-done.1.remote_ref, bf16[2,272,128]{2,1,0:T(8,128)(2,1)S(1)} %pad_maximum_fusion.zero_ref, ...), custom_call_target="tpu_custom_call" | custom-call | tf_op jit(solution)/shard_map/pallas_call | solution.py:44
  68.3 11.3 %all_to_all.25.grad_ref.grads_ref = bf16[8,192,128]{2,1,0:T(8,128)(2,1)S(1)} all-to-all(bf16[8,192,128]{2,1,0:T(8,128)(2,1)S(1)} %shard_map.87), channel_id=1, replica_groups=mesh['z'=16,'y'=4,'x'=4,'core'=2] {'x','core'}, dimensions={0} | all-to-all | bytes 786432 | tf_op jit(solution)/shard_map/all_to_all | solution.py:329
  79.7 3.9 %shard_map.88 = bf16[4,16,40,128]{3,2,1,0:T(8,128)(2,1)} custom-call(f32[1,512]{1,0:T(1,128)S(1)} %convert_element_type.6.target_ref, bf16[8,192,128]{2,1,0:T(8,128)(2,1)S(1)} %all_to_all.25.grad_ref.grads_ref, bf16[896,2048]{1,0:T(8,128)(2,1)} %in_hbm.1), custom_call_target="tpu_custom_call" | custom-call | tf_op jit(solution)/shard_map/pallas_call | solution.py:44
  83.5 14.4 %all_to_all.26.in_ref = bf16[4,16,40,128]{3,2,1,0:T(8,128)(2,1)S(1)} all-to-all(bf16[4,16,40,128]{3,2,1,0:T(8,128)(2,1)} %shard_map.88), channel_id=1, replica_groups=mesh['z'=16,'y'=4,'x'=4,'core'=2] {'y'}, dimensions={0} | all-to-all | bytes 1310720 | tf_op jit(solution)/shard_map/all_to_all | solution.py:329
  98.0 0.8 shard_map.89.after_ref
  98.7 11.7 %all-to-all-start.4 = ((bf16[16,64,128]{2,1,0:T(8,128)(2,1)}), bf16[16,64,128]{2,1,0:T(8,128)(2,1)S(1)}, u32[]{:S(2)}, u32[]{:S(2)}) async-start(bf16[16,64,128]{2,1,0:T(8,128)(2,1)} %shard_map.89.after_ref), calls=%async_computation.4 | async-start | bytes 524288 | tf_op jit(solution)/shard_map/all_to_all | solution.py:329
  110.4 0.7 slice.44
  111.2 16.7 %all-to-all-done.4.returned_ref = bf16[16,64,128]{2,1,0:T(8,128)(2,1)S(1)} async-done(((bf16[16,64,128]{2,1,0:T(8,128)(2,1)}), bf16[16,64,128]{2,1,0:T(8,128)(2,1)S(1)}, u32[]{:S(2)}, u32[]{:S(2)}) %all-to-all-start.4) | async-done | bytes 262176 | tf_op jit(solution)/shard_map/all_to_all | solution.py:329
  127.9 0.8 shard_map.91
  (26 shorter events, 0.9 us)
Async XLA Ops:
  18.6 35.1 %all-to-all-start = ((bf16[64,8,128]{2,1,0:T(8,128)(2,1)}), bf16[64,8,128]{2,1,0:T(8,128)(2,1)S(1)}, u32[]{:S(2)}, u32[]{:S(2)}) async-start(bf16[64,8,128]{2,1,0:T(8,128)(2,1)} %bitcast.14), calls=%async_computation | async-start | bytes 262144 | tf_op jit(solution)/shard_map/all_to_all | solution.py:329
  37.0 5.2 %collective-permute-start = (bf16[4,272,128]{2,1,0:T(8,128)(2,1)}, bf16[4,272,128]{2,1,0:T(8,128)(2,1)S(1)}, u32[]{:S(2)}, u32[]{:S(2)}) collective-permute-start(bf16[4,272,128]{2,1,0:T(8,128)(2,1)} %get-tuple-element.11), channel_id=1, source_target_pairs={{0,1},{1,0},{2,3},{3,2},{4,5},{5,4},{6,7},{7,6},{8,9},{9,8},{10,11... | collective-permute-start | bytes 835592 | tf_op jit(solution)/shard_map/ppermute | solution.py:357
  42.2 16.8 %collective-permute-start.2 = (bf16[2,272,128]{2,1,0:T(8,128)(2,1)S(1)}, bf16[2,272,128]{2,1,0:T(8,128)(2,1)S(1)}, u32[]{:S(2)}, u32[]{:S(2)}) collective-permute-start(bf16[2,272,128]{2,1,0:T(8,128)(2,1)S(1)} %pad_maximum_fusion.2), channel_id=1, source_target_pairs={{0,4},{2,6},{4,0},{6,2},{1,5},{3,7},{5,1},{7,3},{8,12},{10,14},{12... | collective-permute-start | bytes 417800 | tf_op jit(solution)/shard_map/ppermute | solution.py:360
  47.2 11.8 %collective-permute-start.3 = (bf16[2,272,128]{2,1,0:T(8,128)(2,1)S(1)}, bf16[2,272,128]{2,1,0:T(8,128)(2,1)S(1)}, u32[]{:S(2)}, u32[]{:S(2)}) collective-permute-start(bf16[2,272,128]{2,1,0:T(8,128)(2,1)S(1)} %pad_maximum_fusion.3), channel_id=1, source_target_pairs={{0,6},{2,0},{4,2},{6,4},{1,7},{3,1},{5,3},{7,5},{8,14},{10,8},{12,... | collective-permute-start | bytes 417800 | tf_op jit(solution)/shard_map/ppermute | solution.py:360
  50.3 8.7 %collective-permute-start.1 = (bf16[2,272,128]{2,1,0:T(8,128)(2,1)S(1)}, bf16[2,272,128]{2,1,0:T(8,128)(2,1)S(1)}, u32[]{:S(2)}, u32[]{:S(2)}) collective-permute-start(bf16[2,272,128]{2,1,0:T(8,128)(2,1)S(1)} %pad_maximum_fusion.1), channel_id=1, source_target_pairs={{0,2},{2,4},{4,6},{6,0},{1,3},{3,5},{5,7},{7,1},{8,10},{10,12},{12... | collective-permute-start | bytes 417800 | tf_op jit(solution)/shard_map/ppermute | solution.py:360
  54.7 10.1 %all-to-all-start.1 = ((bf16[8,48,128]{2,1,0:T(8,128)(2,1)}), bf16[8,48,128]{2,1,0:T(8,128)(2,1)S(1)}, u32[]{:S(2)}, u32[]{:S(2)}) async-start(bf16[8,48,128]{2,1,0:T(8,128)(2,1)} %shard_map.86), calls=%async_computation.1 | async-start | bytes 196608 | tf_op jit(solution)/shard_map/all_to_all | solution.py:329
  79.6 31.5 %copy-start = (f32[128,128]{1,0:T(8,128)S(1)}, f32[128,128]{1,0:T(8,128)}, u32[]{:S(2)}) copy-start(f32[128,128]{1,0:T(8,128)} %get-tuple-element.12.pair_ref) | copy-start | bytes 196612
  98.7 29.2 %all-to-all-start.4 = ((bf16[16,64,128]{2,1,0:T(8,128)(2,1)}), bf16[16,64,128]{2,1,0:T(8,128)(2,1)S(1)}, u32[]{:S(2)}, u32[]{:S(2)}) async-start(bf16[16,64,128]{2,1,0:T(8,128)(2,1)} %shard_map.89.after_ref), calls=%async_computation.4 | async-start | bytes 524288 | tf_op jit(solution)/shard_map/all_to_all | solution.py:329
where the time goes:
time: 129 us
  starting transfers between devices  47.1 us (37%)
  Pallas kernels  28 us (22%)
  blocking collectives  25.7 us (20%)
  waiting for transfers between devices  22.7 us (18%)
  local copies, waits for them, and re-layouts  3.85 us (3%)
    all_to_all x3, starting transfers between devices, swap(): return lax.all_to_all(array, axis, 0, 0, tiled=True)  34.4 us
    pallas_call x7, Pallas kernels, call(): pl.pallas_call(kernel, out_shape=out_shape, in_specs=specs or [VMEM for _...  28 us
    all_to_all x2, blocking collectives, swap(): return lax.all_to_all(array, axis, 0, 0, tiled=True)  25.7 us
    all_to_all x3, waiting for transfers between devices, swap(): return lax.all_to_all(array, axis, 0, 0, tiled=True)  22.7 us
    ppermute x3, starting transfers between devices, shift(): return lax.ppermute(array, 'x', [(i, (i + k) % 4) for i in range(4)])  10.8 us
  transfers between devices with their start and end apart: 7, of which 3 were waited for; matrix products, arithmetic and copies ran while one was open for 3% of the time, Pallas kernels for 1%

commit v1 on v0

--- a/solution.py
+++ b/solution.py
@@ -36,7 +36,7 @@
 VMEM = pl.BlockSpec(memory_space=pltpu.VMEM)
 HBM = pl.BlockSpec(memory_space=pltpu.HBM)
 GRANT = 12 << 20
-WEIGHT_GRANT = 56_000_000
+WEIGHT_GRANT = 53_000_000
 ALL_VMEM = 67_040_000
 
 
@@ -73,32 +73,29 @@
 
 
 def offer_kernel(
-    sel_hbm, kv_hbm, q_hbm, g_hbm, log_hbm, out_ref, pair_ref, same_hbm, other_hbm, sel_ref, kv_ref, log_ref, term_ref, sems, own_sems
+    sel_hbm, kv_hbm, q_hbm, g_hbm, log_hbm, out_ref, pair_ref, own_ref, *refs
 ):
-    get_sel = pltpu.make_async_copy(sel_hbm, sel_ref, sems.at[0])
-    get_kv = pltpu.make_async_copy(kv_hbm, kv_ref, sems.at[1])
-    get_log = pltpu.make_async_copy(log_hbm, log_ref, sems.at[2])
-    get_sel.start()
-    get_kv.start()
-    get_log.start()
+    block_refs, (sel_ref, kv_ref, q_ref, g_ref, log_ref, term_ref, sems, own_sems) = refs[:4], refs[4:]
+    gets = [
+        pltpu.make_async_copy(hbm, ref, sems.at[i])
+        for i, (hbm, ref) in enumerate(
+            ((sel_hbm, sel_ref), (kv_hbm, kv_ref), (log_hbm, log_ref), (q_hbm, q_ref), (g_hbm, g_ref))
+        )
+    ]
+    for get in gets:
+        get.start()
     x, core = lax.axis_index("x"), lax.axis_index("core")
     places = []
     for k in range(4):
-        for to, side in ((same_hbm, core), (other_hbm, 1 - core)):
+        for j, side in enumerate((core, 1 - core)):
             block = ((x + k) & 3) * 2 + side
-            places.append((to.at[k], pl.multiple_of(jnp.minimum(block, PER - 1) * QB, QB)))
-    copies = []
-    for j, (to, at) in enumerate(places):
-        copies.append(pltpu.make_async_copy(q_hbm.at[pl.ds(at, QB)], to.at[pl.ds(0, QB)], own_sems.at[j, 0]))
-        copies.append(pltpu.make_async_copy(g_hbm.at[pl.ds(at, QB)], to.at[pl.ds(G_AT, QB)], own_sems.at[j, 1]))
-    for copy in copies:
-        copy.start()
+            places.append((block_refs[k].at[j], pl.multiple_of(jnp.minimum(block, PER - 1) * QB, QB)))
     me, member = kv_index(), member_index()
     row = lax.broadcasted_iota(jnp.int32, (128, TOK), 0)
     col = lax.broadcasted_iota(jnp.int32, (128, TOK), 1)
     mine = (row >> 2) * KB + member * PIECE + (row & (PIECE - 1)) == col
     mine = mine.astype(jnp.bfloat16)
-    get_sel.wait()
+    gets[0].wait()
     local = (sel_ref[...] - me * OWN).astype(jnp.float32)
     inside = (local >= 0) & (local < OWN)
     least = jnp.min(jnp.where(inside, local, 1000.0), axis=0, keepdims=True)
@@ -112,7 +109,15 @@
     other = lax.broadcasted_iota(jnp.int32, (KV, 128), 0) != me
     pair_ref[:KV] = jnp.where(other & (least < OWN), least, -1000.0)
     pair_ref[KV:] = jnp.where(other, most, -1000.0)
-    get_log.wait()
+    gets[2].wait()
+    gets[3].wait()
+    gets[4].wait()
+    copies = []
+    for j, (to, at) in enumerate(places):
+        copies.append(pltpu.make_async_copy(q_ref.at[pl.ds(at, QB)], to.at[pl.ds(0, QB)], own_sems.at[j, 0]))
+        copies.append(pltpu.make_async_copy(g_ref.at[pl.ds(at, QB)], to.at[pl.ds(G_AT, QB)], own_sems.at[j, 1]))
+    for copy in copies:
+        copy.start()
     for j, (to, at) in enumerate(places):
         rest = log_ref[:, pl.ds(at, QB)]
         terms = []
@@ -124,7 +129,13 @@
         term_ref[j] = jnp.concatenate(terms, axis=0).astype(jnp.bfloat16)
         copies.append(pltpu.make_async_copy(term_ref.at[j], to.at[pl.ds(LOG_AT, 16)], own_sems.at[j, 2]))
         copies[-1].start()
-    get_kv.wait()
+    gets[1].wait()
+    row = lax.broadcasted_iota(jnp.int32, (QB, QB), 0)
+    turn = ((row >> 2) & 3) * KB + (row >> 4) * PIECE + (row & (PIECE - 1))
+    turn = (turn == lax.broadcasted_iota(jnp.int32, (QB, QB), 1)).astype(jnp.bfloat16)
+    own_at = pl.multiple_of(jnp.minimum(member, PER - 1) * QB, QB)
+    own = jnp.dot(turn, kv_ref[pl.ds(own_at, QB)], preferred_element_type=jnp.float32)
+    own_ref[...] = own.astype(jnp.bfloat16).reshape(TP, DIAG * PIECE, 2 * DH)
     piece = jnp.dot(mine, kv_ref[...], preferred_element_type=jnp.float32).astype(jnp.bfloat16)
     at = lax.broadcasted_iota(jnp.int32, (SLOT_ROWS, 128), 1) - (
         lax.broadcasted_iota(jnp.int32, (SLOT_ROWS, 128), 0) & (PIECE - 1)
@@ -155,8 +166,13 @@
         out_ref[t] = rows[t * ROWS : t * ROWS + REM_ROWS]
 
 
+def mate_kernel(after_ref, zero_ref, one_ref, two_ref, three_ref, out_ref):
+    for k, ref in enumerate((zero_ref, one_ref, two_ref, three_ref)):
+        out_ref[k] = ref[1]
+
+
 def attention_kernel(
-    bias_ref, own_ref, remote_ref, zero_ref, one_ref, two_ref, three_ref, out_ref,
+    bias_ref, own_ref, remote_ref, zero_ref, one_ref, two_ref, three_ref, mate_ref, out_ref,
     kv_ref, in_ref, sum_ref, mask_ref, *pair_refs
 ):
     score_refs, dprob_refs, left_refs = pair_refs[:2], pair_refs[2:4], pair_refs[4:]
@@ -167,7 +183,7 @@
         kv_ref[p * ROWS + REM_ROWS : (p + 1) * ROWS] = own_ref[p]
     for k, ref in enumerate((zero_ref, one_ref, two_ref, three_ref)):
         in_ref[2 * k] = ref[0]
-        in_ref[2 * k + 1] = ref[1]
+        in_ref[2 * k + 1] = mate_ref[k]
     shape = (KEYS, QB)
     key = lax.broadcasted_iota(jnp.int32, shape, 0)
     query = lax.broadcasted_iota(jnp.int32, shape, 1)
@@ -335,32 +351,35 @@
     member = member_index()
     bf16 = jnp.bfloat16
 
-    part = jax.ShapeDtypeStruct((4, SEND, 2 * DH), bf16)
-    offer, pairs, same, other = call(
+    offer, pairs, own, *blocks = call(
         offer_kernel,
-        [jax.ShapeDtypeStruct((SLOTS, 2 * DH), bf16), jax.ShapeDtypeStruct((2 * KV, 128), jnp.float32), part, part],
+        [
+            jax.ShapeDtypeStruct((SLOTS, 2 * DH), bf16),
+            jax.ShapeDtypeStruct((2 * KV, 128), jnp.float32),
+            jax.ShapeDtypeStruct((TP, DIAG * PIECE, 2 * DH), bf16),
+            *[jax.ShapeDtypeStruct((2, SEND, 2 * DH), bf16)] * 4,
+        ],
         [selection.T, keyvals, queries, out_grad, log_sums],
         scratch=[
             pltpu.VMEM((NSEL, KV * PER), jnp.int32),
             pltpu.VMEM((TOK, 2 * DH), bf16),
+            pltpu.VMEM((TOK, 2 * DH), bf16),
+            pltpu.VMEM((TOK, 2 * DH), bf16),
             pltpu.VMEM((2, TOK), jnp.float32),
             pltpu.VMEM((TP, 16, QB), bf16),
-            pltpu.SemaphoreType.DMA((3,)),
+            pltpu.SemaphoreType.DMA((5,)),
             pltpu.SemaphoreType.DMA((TP, 3)),
         ],
         specs=[HBM] * 5,
-        out_specs=[VMEM, VMEM, HBM, HBM],
+        out_specs=[VMEM] * 3 + [HBM] * 4,
         grant=ALL_VMEM,
     )
     fetched = swap(offer.reshape(KV, SLOT_ROWS, 2 * DH), kv_axes)
-
-    other = lax.ppermute(other, "core", [(0, 1), (1, 0)])
 
     def shift(array, k):
         return lax.ppermute(array, "x", [(i, (i + k) % 4) for i in range(4)])
 
-    blocks = [jnp.stack([same[k], other[k]]) for k in range(4)]
-    two, one = shift(blocks[2], 2), shift(blocks[1], 1)
+    two, one, three = shift(blocks[2], 2), shift(blocks[1], 1), shift(blocks[3], 3)
 
     mine = lax.dynamic_slice(selection, (me * PER, 0), (PER, NSEL))[:, DIAG:]
     flat = mine.reshape(-1)
@@ -377,19 +396,21 @@
     live = lax.dynamic_index_in_dim(live, member, 0, keepdims=True)
     bias = jnp.where(live, 0.0, -1e30).astype(jnp.float32)
     bias = jnp.broadcast_to(bias[:, None, :, None], (1, TP, NSEL, PIECE)).reshape(1, KEYS)
-    own_at = jnp.minimum(member, PER - 1) * QB
-    own = lax.dynamic_slice(keyvals, (own_at, 0), (QB, 2 * DH))
-    own = own.reshape(DIAG, TP, PIECE, 2 * DH).transpose(1, 0, 2, 3).reshape(TP, DIAG * PIECE, 2 * DH)
-
     picked = call(
         pick_kernel, jax.ShapeDtypeStruct((TP, REM_ROWS, 2 * DH), bf16), [target, fetched.reshape(SLOTS, 2 * DH)]
     )
     remote = swap(picked, tp_axes)
-    three = shift(blocks[3], 3)
+    mates = call(
+        mate_kernel,
+        jax.ShapeDtypeStruct((4, SEND, 2 * DH), bf16),
+        [picked, blocks[0], one, two, three],
+        specs=[pl.BlockSpec(memory_space=pl.ANY)] + [VMEM] * 4,
+    )
+    mates = lax.ppermute(mates, "core", [(0, 1), (1, 0)])
     grads = call(
         attention_kernel,
         jax.ShapeDtypeStruct((TP, QB + ROWS, 2 * DH), bf16),
-        [bias, own, remote, blocks[0], one, two, three],
+        [bias, own, remote, blocks[0], one, two, three, mates],
         scratch=[
             pltpu.VMEM((KEYS, 2 * DH), bf16),
             pltpu.VMEM((TP, SEND, 2 * DH), bf16),

time: 129 us -> 116 us (0.90)
  Pallas kernels: 28 us -> 11.9 us
  waiting for transfers between devices: 22.7 us -> 26.1 us
    pallas_call x7 -> x8, Pallas kernels: 28 us -> 11.9 us  [call(): pl.pallas_call(kernel, out_shape=out_shape, in_specs=specs or [VMEM for _...]
    all_to_all x3, waiting for transfers between devices: 22.7 us -> 26.1 us  [swap(): return lax.all_to_all(array, axis, 0, 0, tiled=True)]
    unnamed x3 -> x9, local copies, waits for them, and re-layouts: 0.1 us -> 2.66 us
  transfers between devices with their start and end apart: 7 -> 7, of which waited for: 3 -> 3; matrix products, arithmetic and copies ran while one was open for 3% -> 2% of each run, Pallas kernels for 1% -> 1%
where the time goes in v1:
time: 116 us; the launch traced here: 115 us
  starting transfers between devices  46.7 us (40%)
  waiting for transfers between devices  26.1 us (22%)
  blocking collectives  24.7 us (21%)
  Pallas kernels  11.9 us (10%)
  local copies, waits for them, and re-layouts  4.61 us (4%)
    all_to_all x3, starting transfers between devices, swap(): return lax.all_to_all(array, axis, 0, 0, tiled=True)  33.4 us
    all_to_all x3, waiting for transfers between devices, swap(): return lax.all_to_all(array, axis, 0, 0, tiled=True)  26.1 us
    all_to_all x2, blocking collectives, swap(): return lax.all_to_all(array, axis, 0, 0, tiled=True)  24.7 us
    pallas_call x8, Pallas kernels, call(): pl.pallas_call(kernel, out_shape=out_shape, in_specs=specs or [VMEM for _...  11.9 us
    ppermute x3, starting transfers between devices, shift(): return lax.ppermute(array, 'x', [(i, (i + k) % 4) for i in range(4)])  11.4 us
    unnamed x9, local copies, waits for them, and re-layouts  2.66 us
  transfers between devices with their start and end apart: 7, of which 3 were waited for; matrix products, arithmetic and copies ran while one was open for 2% of the time, Pallas kernels for 1%

profile of v1, /device:TPU:32, one launch (start us, length us, event | category | flops | bytes accessed | tf_op | source)
XLA Modules:
  0.0 115.2 jit_solution(16016792704369321613)
XLA Ops:
  0.6 2.9 %shard_map.85 = (bf16[512,128]{1,0:T(8,128)(2,1)}, f32[128,128]{1,0:T(8,128)}, bf16[8,16,128]{2,1,0:T(8,128)(2,1)}, bf16[2,272,128]{2,1,0:T(8,128)(2,1)}, bf16[2...) custom-call(s32[16,448]{1,0:T(8,128)} %bitcast.10, bf16[896,128]{1,0:T(8,128)(2,1)} %kv_hbm.1, ...), custom_call_target="tpu_custom_call" | custom-call | tf_op jit(solution)/shard_map/pallas_call | solution.py:44
  3.6 18.4 %all-to-all-start = ((bf16[64,8,128]{2,1,0:T(8,128)(2,1)}), bf16[64,8,128]{2,1,0:T(8,128)(2,1)S(1)}, u32[]{:S(2)}, u32[]{:S(2)}) async-start(bf16[64,8,128]{2,1,0:T(8,128)(2,1)} %bitcast.9), calls=%async_computation | async-start | bytes 262144 | tf_op jit(solution)/shard_map/all_to_all | solution.py:345
  22.0 3.4 %collective-permute-start = (bf16[2,272,128]{2,1,0:T(8,128)(2,1)}, bf16[2,272,128]{2,1,0:T(8,128)(2,1)S(1)}, u32[]{:S(2)}, u32[]{:S(2)}) collective-permute-start(bf16[2,272,128]{2,1,0:T(8,128)(2,1)} %get-tuple-element.15), channel_id=1, source_target_pairs={{0,2},{2,4},{4,6},{6,0},{1,3},{3,5},{5,7},{7,1},{8,10},{10,12},{12... | collective-permute-start | bytes 417800 | tf_op jit(solution)/shard_map/ppermute | solution.py:380
  25.4 4.6 %collective-permute-start.1 = (bf16[2,272,128]{2,1,0:T(8,128)(2,1)}, bf16[2,272,128]{2,1,0:T(8,128)(2,1)S(1)}, u32[]{:S(2)}, u32[]{:S(2)}) collective-permute-start(bf16[2,272,128]{2,1,0:T(8,128)(2,1)} %get-tuple-element.16), channel_id=1, source_target_pairs={{0,4},{2,6},{4,0},{6,2},{1,5},{3,7},{5,1},{7,3},{8,12},{10,14},{12... | collective-permute-start | bytes 417800 | tf_op jit(solution)/shard_map/ppermute | solution.py:380
  30.0 3.3 %collective-permute-start.2 = (bf16[2,272,128]{2,1,0:T(8,128)(2,1)}, bf16[2,272,128]{2,1,0:T(8,128)(2,1)S(1)}, u32[]{:S(2)}, u32[]{:S(2)}) collective-permute-start(bf16[2,272,128]{2,1,0:T(8,128)(2,1)} %get-tuple-element.17), channel_id=1, source_target_pairs={{0,6},{2,0},{4,2},{6,4},{1,7},{3,1},{5,3},{7,5},{8,14},{10,8},{12,... | collective-permute-start | bytes 417800 | tf_op jit(solution)/shard_map/ppermute | solution.py:380
  33.4 0.8 dynamic-slice
  34.4 0.2 select_reduce_fusion
  34.9 3.8 %all-to-all-done = bf16[64,8,128]{2,1,0:T(8,128)(2,1)S(1)} async-done(((bf16[64,8,128]{2,1,0:T(8,128)(2,1)}), bf16[64,8,128]{2,1,0:T(8,128)(2,1)S(1)}, u32[]{:S(2)}, u32[]{:S(2)}) %all-to-all-start) | async-done | bytes 131104 | tf_op jit(solution)/shard_map/all_to_all | solution.py:345
  38.7 1.0 shard_map.86.after_ref
  39.7 0.9 copy-done
  40.6 1.9 %collective-permute-start.3 = (bf16[4,272,128]{2,1,0:T(8,128)(2,1)S(1)}, bf16[4,272,128]{2,1,0:T(8,128)(2,1)S(1)}, u32[]{:S(2)}, u32[]{:S(2)}) collective-permute-start(bf16[4,272,128]{2,1,0:T(8,128)(2,1)S(1)} %shard_map.87), channel_id=1, source_target_pairs={{0,1},{1,0},{2,3},{3,2},{4,5},{5,4},{6,7},{7,6},{8,9},{9,8},{10,11... | collective-permute-start | bytes 835592 | tf_op jit(solution)/shard_map/ppermute | solution.py:409
  42.6 4.4 %all-to-all-start.1 = ((bf16[8,48,128]{2,1,0:T(8,128)(2,1)}), bf16[8,48,128]{2,1,0:T(8,128)(2,1)S(1)}, u32[]{:S(2)}, u32[]{:S(2)}) async-start(bf16[8,48,128]{2,1,0:T(8,128)(2,1)} %shard_map.86.after_ref), calls=%async_computation.1 | async-start | bytes 196608 | tf_op jit(solution)/shard_map/all_to_all | solution.py:345
  47.2 5.6 %all-to-all-done.1.remote_ref = bf16[8,48,128]{2,1,0:T(8,128)(2,1)S(1)} async-done(((bf16[8,48,128]{2,1,0:T(8,128)(2,1)}), bf16[8,48,128]{2,1,0:T(8,128)(2,1)S(1)}, u32[]{:S(2)}, u32[]{:S(2)}) %all-to-all-start.1) | async-done | bytes 98336 | tf_op jit(solution)/shard_map/all_to_all | solution.py:345
  52.8 0.9 copy-done.1
  53.8 0.8 copy-done.3
  54.5 3.6 %shard_map.88 = bf16[8,192,128]{2,1,0:T(8,128)(2,1)S(1)} custom-call(f32[1,512]{1,0:T(1,128)S(1)} %broadcast_in_dim.54.bias_ref, bf16[8,16,128]{2,1,0:T(8,128)(2,1)S(1)} %copy-done.3, bf16[8,48,128]{2,1,0:T(8,128)(2,1)S(1)} %all-to-all-done.1.remote_ref, bf16[2,272,128]{2,1,0:T(8,128)(2,1)S(1)} %copy-done.1, ...), custom_call_target="tpu_custom_call" | custom-call | tf_op jit(solution)/shard_map/pallas_call | solution.py:44
  58.1 11.3 %all_to_all.25.grad_ref.grads_ref = bf16[8,192,128]{2,1,0:T(8,128)(2,1)S(1)} all-to-all(bf16[8,192,128]{2,1,0:T(8,128)(2,1)S(1)} %shard_map.88), channel_id=1, replica_groups=mesh['z'=16,'y'=4,'x'=4,'core'=2] {'x','core'}, dimensions={0} | all-to-all | bytes 786432 | tf_op jit(solution)/shard_map/all_to_all | solution.py:345
  69.4 2.8 %shard_map.89 = bf16[4,16,40,128]{3,2,1,0:T(8,128)(2,1)S(1)} custom-call(f32[1,512]{1,0:T(1,128)S(1)} %convert_element_type.6.target_ref, bf16[8,192,128]{2,1,0:T(8,128)(2,1)S(1)} %all_to_all.25.grad_ref.grads_ref, bf16[896,2048]{1,0:T(8,128)(2,1)} %in_hbm.1), custom_call_target="tpu_custom_call" | custom-call | tf_op jit(solution)/shard_map/pallas_call | solution.py:44
  72.2 13.4 %all_to_all.26.in_ref = bf16[4,16,40,128]{3,2,1,0:T(8,128)(2,1)S(1)} all-to-all(bf16[4,16,40,128]{3,2,1,0:T(8,128)(2,1)S(1)} %shard_map.89), channel_id=1, replica_groups=mesh['z'=16,'y'=4,'x'=4,'core'=2] {'y'}, dimensions={0} | all-to-all | bytes 1310720 | tf_op jit(solution)/shard_map/all_to_all | solution.py:345
  85.6 0.8 shard_map.90.after_ref
  86.3 10.6 %all-to-all-start.4 = ((bf16[16,64,128]{2,1,0:T(8,128)(2,1)}), bf16[16,64,128]{2,1,0:T(8,128)(2,1)S(1)}, u32[]{:S(2)}, u32[]{:S(2)}) async-start(bf16[16,64,128]{2,1,0:T(8,128)(2,1)} %shard_map.90.after_ref), calls=%async_computation.4 | async-start | bytes 524288 | tf_op jit(solution)/shard_map/all_to_all | solution.py:345
  96.9 0.7 slice.8
  97.7 16.7 %all-to-all-done.4.returned_ref = bf16[16,64,128]{2,1,0:T(8,128)(2,1)S(1)} async-done(((bf16[16,64,128]{2,1,0:T(8,128)(2,1)}), bf16[16,64,128]{2,1,0:T(8,128)(2,1)S(1)}, u32[]{:S(2)}, u32[]{:S(2)}) %all-to-all-start.4) | async-done | bytes 262176 | tf_op jit(solution)/shard_map/all_to_all | solution.py:345
  114.4 0.8 shard_map.92
  (25 shorter events, 0.9 us)
Async XLA Ops:
  3.6 35.1 %all-to-all-start = ((bf16[64,8,128]{2,1,0:T(8,128)(2,1)}), bf16[64,8,128]{2,1,0:T(8,128)(2,1)S(1)}, u32[]{:S(2)}, u32[]{:S(2)}) async-start(bf16[64,8,128]{2,1,0:T(8,128)(2,1)} %bitcast.9), calls=%async_computation | async-start | bytes 262144 | tf_op jit(solution)/shard_map/all_to_all | solution.py:345
  22.0 17.7 %collective-permute-start = (bf16[2,272,128]{2,1,0:T(8,128)(2,1)}, bf16[2,272,128]{2,1,0:T(8,128)(2,1)S(1)}, u32[]{:S(2)}, u32[]{:S(2)}) collective-permute-start(bf16[2,272,128]{2,1,0:T(8,128)(2,1)} %get-tuple-element.15), channel_id=1, source_target_pairs={{0,2},{2,4},{4,6},{6,0},{1,3},{3,5},{5,7},{7,1},{8,10},{10,12},{12... | collective-permute-start | bytes 417800 | tf_op jit(solution)/shard_map/ppermute | solution.py:380
  25.4 14.3 %collective-permute-start.1 = (bf16[2,272,128]{2,1,0:T(8,128)(2,1)}, bf16[2,272,128]{2,1,0:T(8,128)(2,1)S(1)}, u32[]{:S(2)}, u32[]{:S(2)}) collective-permute-start(bf16[2,272,128]{2,1,0:T(8,128)(2,1)} %get-tuple-element.16), channel_id=1, source_target_pairs={{0,4},{2,6},{4,0},{6,2},{1,5},{3,7},{5,1},{7,3},{8,12},{10,14},{12... | collective-permute-start | bytes 417800 | tf_op jit(solution)/shard_map/ppermute | solution.py:380
  30.0 9.7 %collective-permute-start.2 = (bf16[2,272,128]{2,1,0:T(8,128)(2,1)}, bf16[2,272,128]{2,1,0:T(8,128)(2,1)S(1)}, u32[]{:S(2)}, u32[]{:S(2)}) collective-permute-start(bf16[2,272,128]{2,1,0:T(8,128)(2,1)} %get-tuple-element.17), channel_id=1, source_target_pairs={{0,6},{2,0},{4,2},{6,4},{1,7},{3,1},{5,3},{7,5},{8,14},{10,8},{12,... | collective-permute-start | bytes 417800 | tf_op jit(solution)/shard_map/ppermute | solution.py:380
  39.7 0.9 copy-start
  40.6 12.2 %collective-permute-start.3 = (bf16[4,272,128]{2,1,0:T(8,128)(2,1)S(1)}, bf16[4,272,128]{2,1,0:T(8,128)(2,1)S(1)}, u32[]{:S(2)}, u32[]{:S(2)}) collective-permute-start(bf16[4,272,128]{2,1,0:T(8,128)(2,1)S(1)} %shard_map.87), channel_id=1, source_target_pairs={{0,1},{1,0},{2,3},{3,2},{4,5},{5,4},{6,7},{7,6},{8,9},{9,8},{10,11... | collective-permute-start | bytes 835592 | tf_op jit(solution)/shard_map/ppermute | solution.py:409
  42.6 10.2 %all-to-all-start.1 = ((bf16[8,48,128]{2,1,0:T(8,128)(2,1)}), bf16[8,48,128]{2,1,0:T(8,128)(2,1)S(1)}, u32[]{:S(2)}, u32[]{:S(2)}) async-start(bf16[8,48,128]{2,1,0:T(8,128)(2,1)} %shard_map.86.after_ref), calls=%async_computation.1 | async-start | bytes 196608 | tf_op jit(solution)/shard_map/all_to_all | solution.py:345
  52.8 0.9 copy-start.1
  53.7 0.8 copy-start.3
  69.4 28.2 %copy-start.2 = (f32[128,128]{1,0:T(8,128)S(1)}, f32[128,128]{1,0:T(8,128)}, u32[]{:S(2)}) copy-start(f32[128,128]{1,0:T(8,128)} %get-tuple-element.18.pair_ref) | copy-start | bytes 196612
  86.3 28.0 %all-to-all-start.4 = ((bf16[16,64,128]{2,1,0:T(8,128)(2,1)}), bf16[16,64,128]{2,1,0:T(8,128)(2,1)S(1)}, u32[]{:S(2)}, u32[]{:S(2)}) async-start(bf16[16,64,128]{2,1,0:T(8,128)(2,1)} %shard_map.90.after_ref), calls=%async_computation.4 | async-start | bytes 524288 | tf_op jit(solution)/shard_map/all_to_all | solution.py:345

commit v2 on v1

--- a/solution.py
+++ b/solution.py
@@ -118,16 +118,18 @@
         copies.append(pltpu.make_async_copy(g_ref.at[pl.ds(at, QB)], to.at[pl.ds(G_AT, QB)], own_sems.at[j, 1]))
     for copy in copies:
         copy.start()
+    rest = log_ref[...]
+    terms = []
+    for _ in range(3):
+        term = rest.astype(jnp.bfloat16).astype(jnp.float32)
+        terms.append(term)
+        rest = rest - term
+    terms.append(jnp.zeros((10, TOK), jnp.float32))
+    term_ref[...] = jnp.concatenate(terms, axis=0).astype(jnp.bfloat16)
     for j, (to, at) in enumerate(places):
-        rest = log_ref[:, pl.ds(at, QB)]
-        terms = []
-        for _ in range(3):
-            term = rest.astype(jnp.bfloat16).astype(jnp.float32)
-            terms.append(term)
-            rest = rest - term
-        terms.append(jnp.zeros((10, QB), jnp.float32))
-        term_ref[j] = jnp.concatenate(terms, axis=0).astype(jnp.bfloat16)
-        copies.append(pltpu.make_async_copy(term_ref.at[j], to.at[pl.ds(LOG_AT, 16)], own_sems.at[j, 2]))
+        copies.append(
+            pltpu.make_async_copy(term_ref.at[:, pl.ds(at, QB)], to.at[pl.ds(LOG_AT, 16)], own_sems.at[j, 2])
+        )
         copies[-1].start()
     gets[1].wait()
     row = lax.broadcasted_iota(jnp.int32, (QB, QB), 0)
@@ -166,7 +168,9 @@
         out_ref[t] = rows[t * ROWS : t * ROWS + REM_ROWS]
 
 
-def mate_kernel(after_ref, zero_ref, one_ref, two_ref, three_ref, out_ref):
+def mate_kernel(after_ref, given_ref, zero_ref, one_ref, two_ref, three_ref, out_ref, kept_ref, own_ref):
+    kept_ref[...] = zero_ref[0]
+    own_ref[...] = given_ref[...]
     for k, ref in enumerate((zero_ref, one_ref, two_ref, three_ref)):
         out_ref[k] = ref[1]
 
@@ -182,7 +186,7 @@
         kv_ref[p * ROWS : p * ROWS + REM_ROWS] = remote_ref[p]
         kv_ref[p * ROWS + REM_ROWS : (p + 1) * ROWS] = own_ref[p]
     for k, ref in enumerate((zero_ref, one_ref, two_ref, three_ref)):
-        in_ref[2 * k] = ref[0]
+        in_ref[2 * k] = ref[0] if k else ref[...]
         in_ref[2 * k + 1] = mate_ref[k]
     shape = (KEYS, QB)
     key = lax.broadcasted_iota(jnp.int32, shape, 0)
@@ -366,7 +370,7 @@
             pltpu.VMEM((TOK, 2 * DH), bf16),
             pltpu.VMEM((TOK, 2 * DH), bf16),
             pltpu.VMEM((2, TOK), jnp.float32),
-            pltpu.VMEM((TP, 16, QB), bf16),
+            pltpu.VMEM((16, TOK), bf16),
             pltpu.SemaphoreType.DMA((5,)),
             pltpu.SemaphoreType.DMA((TP, 3)),
         ],
@@ -400,17 +404,21 @@
         pick_kernel, jax.ShapeDtypeStruct((TP, REM_ROWS, 2 * DH), bf16), [target, fetched.reshape(SLOTS, 2 * DH)]
     )
     remote = swap(picked, tp_axes)
-    mates = call(
+    mates, kept, own = call(
         mate_kernel,
-        jax.ShapeDtypeStruct((4, SEND, 2 * DH), bf16),
-        [picked, blocks[0], one, two, three],
-        specs=[pl.BlockSpec(memory_space=pl.ANY)] + [VMEM] * 4,
+        [
+            jax.ShapeDtypeStruct((4, SEND, 2 * DH), bf16),
+            jax.ShapeDtypeStruct((SEND, 2 * DH), bf16),
+            jax.ShapeDtypeStruct((TP, DIAG * PIECE, 2 * DH), bf16),
+        ],
+        [picked, own, blocks[0], one, two, three],
+        specs=[pl.BlockSpec(memory_space=pl.ANY)] + [VMEM] * 5,
     )
     mates = lax.ppermute(mates, "core", [(0, 1), (1, 0)])
     grads = call(
         attention_kernel,
         jax.ShapeDtypeStruct((TP, QB + ROWS, 2 * DH), bf16),
-        [bias, own, remote, blocks[0], one, two, three, mates],
+        [bias, own, remote, kept, one, two, three, mates],
         scratch=[
             pltpu.VMEM((KEYS, 2 * DH), bf16),
             pltpu.VMEM((TP, SEND, 2 * DH), bf16),

time: 116 us -> 115 us (level)
    unnamed x9 -> x7, local copies, waits for them, and re-layouts: 2.66 us -> 1.76 us
where the time goes in v2:
time: 115 us; the launch traced here: 114 us
  starting transfers between devices  46.7 us (41%)
  waiting for transfers between devices  26.1 us (23%)
  blocking collectives  24.7 us (21%)
  Pallas kernels  12 us (10%)
  local copies, waits for them, and re-layouts  3.71 us (3%)
    all_to_all x3, starting transfers between devices, swap(): return lax.all_to_all(array, axis, 0, 0, tiled=True)  33.4 us
    all_to_all x3, waiting for transfers between devices, swap(): return lax.all_to_all(array, axis, 0, 0, tiled=True)  26.1 us
    all_to_all x2, blocking collectives, swap(): return lax.all_to_all(array, axis, 0, 0, tiled=True)  24.7 us
    pallas_call x8, Pallas kernels, call(): pl.pallas_call(kernel, out_shape=out_shape, in_specs=specs or [VMEM for _...  12 us
    ppermute x3, starting transfers between devices, shift(): return lax.ppermute(array, 'x', [(i, (i + k) % 4) for i in range(4)])  11.4 us
  transfers between devices with their start and end apart: 7, of which 3 were waited for; matrix products, arithmetic and copies ran while one was open for 2% of the time, Pallas kernels for 1%

profile of v2, /device:TPU:32, one launch (start us, length us, event | category | flops | bytes accessed | tf_op | source)
XLA Modules:
  0.0 114.3 jit_solution(17683420681611916247)
XLA Ops:
  0.6 2.9 %shard_map.85 = (bf16[512,128]{1,0:T(8,128)(2,1)}, f32[128,128]{1,0:T(8,128)}, bf16[8,16,128]{2,1,0:T(8,128)(2,1)}, bf16[2,272,128]{2,1,0:T(8,128)(2,1)}, bf16[2...) custom-call(s32[16,448]{1,0:T(8,128)} %bitcast.10, bf16[896,128]{1,0:T(8,128)(2,1)} %kv_hbm.1, ...), custom_call_target="tpu_custom_call" | custom-call | tf_op jit(solution)/shard_map/pallas_call | solution.py:44
  3.6 18.4 %all-to-all-start = ((bf16[64,8,128]{2,1,0:T(8,128)(2,1)}), bf16[64,8,128]{2,1,0:T(8,128)(2,1)S(1)}, u32[]{:S(2)}, u32[]{:S(2)}) async-start(bf16[64,8,128]{2,1,0:T(8,128)(2,1)} %bitcast.9), calls=%async_computation | async-start | bytes 262144 | tf_op jit(solution)/shard_map/all_to_all | solution.py:349
  22.0 3.4 %collective-permute-start = (bf16[2,272,128]{2,1,0:T(8,128)(2,1)}, bf16[2,272,128]{2,1,0:T(8,128)(2,1)S(1)}, u32[]{:S(2)}, u32[]{:S(2)}) collective-permute-start(bf16[2,272,128]{2,1,0:T(8,128)(2,1)} %get-tuple-element.18), channel_id=1, source_target_pairs={{0,2},{2,4},{4,6},{6,0},{1,3},{3,5},{5,7},{7,1},{8,10},{10,12},{12... | collective-permute-start | bytes 417800 | tf_op jit(solution)/shard_map/ppermute | solution.py:384
  25.4 4.6 %collective-permute-start.1 = (bf16[2,272,128]{2,1,0:T(8,128)(2,1)}, bf16[2,272,128]{2,1,0:T(8,128)(2,1)S(1)}, u32[]{:S(2)}, u32[]{:S(2)}) collective-permute-start(bf16[2,272,128]{2,1,0:T(8,128)(2,1)} %get-tuple-element.19), channel_id=1, source_target_pairs={{0,4},{2,6},{4,0},{6,2},{1,5},{3,7},{5,1},{7,3},{8,12},{10,14},{12... | collective-permute-start | bytes 417800 | tf_op jit(solution)/shard_map/ppermute | solution.py:384
  30.0 3.3 %collective-permute-start.2 = (bf16[2,272,128]{2,1,0:T(8,128)(2,1)}, bf16[2,272,128]{2,1,0:T(8,128)(2,1)S(1)}, u32[]{:S(2)}, u32[]{:S(2)}) collective-permute-start(bf16[2,272,128]{2,1,0:T(8,128)(2,1)} %get-tuple-element.20), channel_id=1, source_target_pairs={{0,6},{2,0},{4,2},{6,4},{1,7},{3,1},{5,3},{7,5},{8,14},{10,8},{12,... | collective-permute-start | bytes 417800 | tf_op jit(solution)/shard_map/ppermute | solution.py:384
  33.4 0.8 dynamic-slice
  34.4 0.2 select_reduce_fusion
  34.9 3.8 %all-to-all-done = bf16[64,8,128]{2,1,0:T(8,128)(2,1)S(1)} async-done(((bf16[64,8,128]{2,1,0:T(8,128)(2,1)}), bf16[64,8,128]{2,1,0:T(8,128)(2,1)S(1)}, u32[]{:S(2)}, u32[]{:S(2)}) %all-to-all-start) | async-done | bytes 131104 | tf_op jit(solution)/shard_map/all_to_all | solution.py:349
  38.7 1.0 shard_map.86.after_ref
  39.7 0.9 copy-done
  40.6 0.8 copy-done.2
  41.4 1.9 %collective-permute-start.3 = (bf16[4,272,128]{2,1,0:T(8,128)(2,1)S(1)}, bf16[4,272,128]{2,1,0:T(8,128)(2,1)S(1)}, u32[]{:S(2)}, u32[]{:S(2)}) collective-permute-start(bf16[4,272,128]{2,1,0:T(8,128)(2,1)S(1)} %get-tuple-element.23), channel_id=1, source_target_pairs={{0,1},{1,0},{2,3},{3,2},{4,5},{5,4},{6,7},{7,6},{8,9},{9,8},{10,11... | collective-permute-start | bytes 835592 | tf_op jit(solution)/shard_map/ppermute | solution.py:417
  43.4 4.4 %all-to-all-start.1 = ((bf16[8,48,128]{2,1,0:T(8,128)(2,1)}), bf16[8,48,128]{2,1,0:T(8,128)(2,1)S(1)}, u32[]{:S(2)}, u32[]{:S(2)}) async-start(bf16[8,48,128]{2,1,0:T(8,128)(2,1)} %shard_map.86.after_ref), calls=%async_computation.1 | async-start | bytes 196608 | tf_op jit(solution)/shard_map/all_to_all | solution.py:349
  47.9 0.1 broadcast_in_dim.54.bias_ref
  48.0 5.6 %all-to-all-done.1.remote_ref = bf16[8,48,128]{2,1,0:T(8,128)(2,1)S(1)} async-done(((bf16[8,48,128]{2,1,0:T(8,128)(2,1)}), bf16[8,48,128]{2,1,0:T(8,128)(2,1)S(1)}, u32[]{:S(2)}, u32[]{:S(2)}) %all-to-all-start.1) | async-done | bytes 98336 | tf_op jit(solution)/shard_map/all_to_all | solution.py:349
  53.6 3.6 %shard_map.88 = bf16[8,192,128]{2,1,0:T(8,128)(2,1)S(1)} custom-call(f32[1,512]{1,0:T(1,128)S(1)} %broadcast_in_dim.54.bias_ref, bf16[8,16,128]{2,1,0:T(8,128)(2,1)S(1)} %get-tuple-element.21.own_ref, bf16[8,48,128]{2,1,0:T(8,128)(2,1)S(1)} %all-to-all-done.1.remote_ref, bf16[272,128]{1,0:T(8,128)(2,1)S(1)} %get-tuple-element.22.zero_ref, ...), custom_call_target="tpu_custom_call" | custom-call | tf_op jit(solution)/shard_map/pallas_call | solution.py:44
  57.2 11.3 %all_to_all.25.grad_ref.grads_ref = bf16[8,192,128]{2,1,0:T(8,128)(2,1)S(1)} all-to-all(bf16[8,192,128]{2,1,0:T(8,128)(2,1)S(1)} %shard_map.88), channel_id=1, replica_groups=mesh['z'=16,'y'=4,'x'=4,'core'=2] {'x','core'}, dimensions={0} | all-to-all | bytes 786432 | tf_op jit(solution)/shard_map/all_to_all | solution.py:349
  68.5 2.8 %shard_map.89 = bf16[4,16,40,128]{3,2,1,0:T(8,128)(2,1)S(1)} custom-call(f32[1,512]{1,0:T(1,128)S(1)} %convert_element_type.6.target_ref, bf16[8,192,128]{2,1,0:T(8,128)(2,1)S(1)} %all_to_all.25.grad_ref.grads_ref, bf16[896,2048]{1,0:T(8,128)(2,1)} %in_hbm.1), custom_call_target="tpu_custom_call" | custom-call | tf_op jit(solution)/shard_map/pallas_call | solution.py:44
  71.3 13.4 %all_to_all.26.in_ref = bf16[4,16,40,128]{3,2,1,0:T(8,128)(2,1)S(1)} all-to-all(bf16[4,16,40,128]{3,2,1,0:T(8,128)(2,1)S(1)} %shard_map.89), channel_id=1, replica_groups=mesh['z'=16,'y'=4,'x'=4,'core'=2] {'y'}, dimensions={0} | all-to-all | bytes 1310720 | tf_op jit(solution)/shard_map/all_to_all | solution.py:349
  84.7 0.8 shard_map.90.after_ref
  85.4 10.6 %all-to-all-start.4 = ((bf16[16,64,128]{2,1,0:T(8,128)(2,1)}), bf16[16,64,128]{2,1,0:T(8,128)(2,1)S(1)}, u32[]{:S(2)}, u32[]{:S(2)}) async-start(bf16[16,64,128]{2,1,0:T(8,128)(2,1)} %shard_map.90.after_ref), calls=%async_computation.4 | async-start | bytes 524288 | tf_op jit(solution)/shard_map/all_to_all | solution.py:349
  96.0 0.7 slice.8
  96.8 16.7 %all-to-all-done.4.returned_ref = bf16[16,64,128]{2,1,0:T(8,128)(2,1)S(1)} async-done(((bf16[16,64,128]{2,1,0:T(8,128)(2,1)}), bf16[16,64,128]{2,1,0:T(8,128)(2,1)S(1)}, u32[]{:S(2)}, u32[]{:S(2)}) %all-to-all-start.4) | async-done | bytes 262176 | tf_op jit(solution)/shard_map/all_to_all | solution.py:349
  113.5 0.8 shard_map.92
  (23 shorter events, 0.8 us)
Async XLA Ops:
  3.6 35.1 %all-to-all-start = ((bf16[64,8,128]{2,1,0:T(8,128)(2,1)}), bf16[64,8,128]{2,1,0:T(8,128)(2,1)S(1)}, u32[]{:S(2)}, u32[]{:S(2)}) async-start(bf16[64,8,128]{2,1,0:T(8,128)(2,1)} %bitcast.9), calls=%async_computation | async-start | bytes 262144 | tf_op jit(solution)/shard_map/all_to_all | solution.py:349
  22.0 17.7 %collective-permute-start = (bf16[2,272,128]{2,1,0:T(8,128)(2,1)}, bf16[2,272,128]{2,1,0:T(8,128)(2,1)S(1)}, u32[]{:S(2)}, u32[]{:S(2)}) collective-permute-start(bf16[2,272,128]{2,1,0:T(8,128)(2,1)} %get-tuple-element.18), channel_id=1, source_target_pairs={{0,2},{2,4},{4,6},{6,0},{1,3},{3,5},{5,7},{7,1},{8,10},{10,12},{12... | collective-permute-start | bytes 417800 | tf_op jit(solution)/shard_map/ppermute | solution.py:384
  25.4 14.3 %collective-permute-start.1 = (bf16[2,272,128]{2,1,0:T(8,128)(2,1)}, bf16[2,272,128]{2,1,0:T(8,128)(2,1)S(1)}, u32[]{:S(2)}, u32[]{:S(2)}) collective-permute-start(bf16[2,272,128]{2,1,0:T(8,128)(2,1)} %get-tuple-element.19), channel_id=1, source_target_pairs={{0,4},{2,6},{4,0},{6,2},{1,5},{3,7},{5,1},{7,3},{8,12},{10,14},{12... | collective-permute-start | bytes 417800 | tf_op jit(solution)/shard_map/ppermute | solution.py:384
  30.0 9.7 %collective-permute-start.2 = (bf16[2,272,128]{2,1,0:T(8,128)(2,1)}, bf16[2,272,128]{2,1,0:T(8,128)(2,1)S(1)}, u32[]{:S(2)}, u32[]{:S(2)}) collective-permute-start(bf16[2,272,128]{2,1,0:T(8,128)(2,1)} %get-tuple-element.20), channel_id=1, source_target_pairs={{0,6},{2,0},{4,2},{6,4},{1,7},{3,1},{5,3},{7,5},{8,14},{10,8},{12,... | collective-permute-start | bytes 417800 | tf_op jit(solution)/shard_map/ppermute | solution.py:384
  39.7 0.9 copy-start
  40.6 0.8 copy-start.2
  41.4 12.2 %collective-permute-start.3 = (bf16[4,272,128]{2,1,0:T(8,128)(2,1)S(1)}, bf16[4,272,128]{2,1,0:T(8,128)(2,1)S(1)}, u32[]{:S(2)}, u32[]{:S(2)}) collective-permute-start(bf16[4,272,128]{2,1,0:T(8,128)(2,1)S(1)} %get-tuple-element.23), channel_id=1, source_target_pairs={{0,1},{1,0},{2,3},{3,2},{4,5},{5,4},{6,7},{7,6},{8,9},{9,8},{10,11... | collective-permute-start | bytes 835592 | tf_op jit(solution)/shard_map/ppermute | solution.py:417
  43.4 10.2 %all-to-all-start.1 = ((bf16[8,48,128]{2,1,0:T(8,128)(2,1)}), bf16[8,48,128]{2,1,0:T(8,128)(2,1)S(1)}, u32[]{:S(2)}, u32[]{:S(2)}) async-start(bf16[8,48,128]{2,1,0:T(8,128)(2,1)} %shard_map.86.after_ref), calls=%async_computation.1 | async-start | bytes 196608 | tf_op jit(solution)/shard_map/all_to_all | solution.py:349
  68.5 28.2 %copy-start.1 = (f32[128,128]{1,0:T(8,128)S(1)}, f32[128,128]{1,0:T(8,128)}, u32[]{:S(2)}) copy-start(f32[128,128]{1,0:T(8,128)} %get-tuple-element.24.pair_ref) | copy-start | bytes 196612
  85.4 28.1 %all-to-all-start.4 = ((bf16[16,64,128]{2,1,0:T(8,128)(2,1)}), bf16[16,64,128]{2,1,0:T(8,128)(2,1)S(1)}, u32[]{:S(2)}, u32[]{:S(2)}) async-start(bf16[16,64,128]{2,1,0:T(8,128)(2,1)} %shard_map.90.after_ref), calls=%async_computation.4 | async-start | bytes 524288 | tf_op jit(solution)/shard_map/all_to_all | solution.py:349

commit v3 on v2

--- a/solution.py
+++ b/solution.py
@@ -109,6 +109,15 @@
     other = lax.broadcasted_iota(jnp.int32, (KV, 128), 0) != me
     pair_ref[:KV] = jnp.where(other & (least < OWN), least, -1000.0)
     pair_ref[KV:] = jnp.where(other, most, -1000.0)
+    gets[1].wait()
+    piece = jnp.dot(mine, kv_ref[...], preferred_element_type=jnp.float32).astype(jnp.bfloat16)
+    at = lax.broadcasted_iota(jnp.int32, (SLOT_ROWS, 128), 1) - (
+        lax.broadcasted_iota(jnp.int32, (SLOT_ROWS, 128), 0) & (PIECE - 1)
+    )
+    at = jnp.where((at & (PIECE - 1)) == 0, at >> 2, -1).astype(jnp.float32)
+    onehot = slot_blocks(pair_ref).reshape(KV, SLOT_ROWS, 128) == at[None]
+    onehot = onehot.reshape(SLOTS, 128).astype(jnp.bfloat16)
+    out_ref[...] = jnp.dot(onehot, piece, preferred_element_type=jnp.float32).astype(jnp.bfloat16)
     gets[2].wait()
     gets[3].wait()
     gets[4].wait()
@@ -131,21 +140,12 @@
             pltpu.make_async_copy(term_ref.at[:, pl.ds(at, QB)], to.at[pl.ds(LOG_AT, 16)], own_sems.at[j, 2])
         )
         copies[-1].start()
-    gets[1].wait()
     row = lax.broadcasted_iota(jnp.int32, (QB, QB), 0)
     turn = ((row >> 2) & 3) * KB + (row >> 4) * PIECE + (row & (PIECE - 1))
     turn = (turn == lax.broadcasted_iota(jnp.int32, (QB, QB), 1)).astype(jnp.bfloat16)
     own_at = pl.multiple_of(jnp.minimum(member, PER - 1) * QB, QB)
     own = jnp.dot(turn, kv_ref[pl.ds(own_at, QB)], preferred_element_type=jnp.float32)
     own_ref[...] = own.astype(jnp.bfloat16).reshape(TP, DIAG * PIECE, 2 * DH)
-    piece = jnp.dot(mine, kv_ref[...], preferred_element_type=jnp.float32).astype(jnp.bfloat16)
-    at = lax.broadcasted_iota(jnp.int32, (SLOT_ROWS, 128), 1) - (
-        lax.broadcasted_iota(jnp.int32, (SLOT_ROWS, 128), 0) & (PIECE - 1)
-    )
-    at = jnp.where((at & (PIECE - 1)) == 0, at >> 2, -1).astype(jnp.float32)
-    onehot = slot_blocks(pair_ref).reshape(KV, SLOT_ROWS, 128) == at[None]
-    onehot = onehot.reshape(SLOTS, 128).astype(jnp.bfloat16)
-    out_ref[...] = jnp.dot(onehot, piece, preferred_element_type=jnp.float32).astype(jnp.bfloat16)
     for copy in copies:
         copy.wait()
 
@@ -176,7 +176,7 @@
 
 
 def attention_kernel(
-    bias_ref, own_ref, remote_ref, zero_ref, one_ref, two_ref, three_ref, mate_ref, out_ref,
+    after_ref, bias_ref, own_ref, remote_ref, zero_ref, one_ref, two_ref, three_ref, mate_ref, out_ref,
     kv_ref, in_ref, sum_ref, mask_ref, *pair_refs
 ):
     score_refs, dprob_refs, left_refs = pair_refs[:2], pair_refs[2:4], pair_refs[4:]
@@ -268,12 +268,18 @@
 CHUNK = 256
 
 
-def weight_kernel(target_ref, grad_ref, in_hbm, out_ref, in_ref, turned_ref, sum_ref, sems):
+def weight_kernel(target_ref, grad_ref, in_hbm, out_ref, query_hbm, in_ref, turned_ref, sum_ref, sems, out_sems):
     copies = []
     for t in range(PER):
         rows = pl.ds(t * QB, QB)
         copies.append(pltpu.make_async_copy(in_hbm.at[rows], in_ref.at[rows], sems.at[t]))
         copies[-1].start()
+    leaving = [
+        pltpu.make_async_copy(grad_ref.at[t, pl.ds(0, QB)], query_hbm.at[pl.ds(t * QB, QB)], out_sems.at[t])
+        for t in range(PER)
+    ]
+    for copy in leaving:
+        copy.start()
     row = lax.broadcasted_iota(jnp.int32, (SLOTS, KEYS), 0).astype(jnp.float32)
     onehot = (row == target_ref[...]).astype(jnp.bfloat16)
     entries = jnp.concatenate([grad_ref[t, QB:] for t in range(TP)], axis=0)
@@ -303,20 +309,27 @@
                     at = half * 128 + d * W_ROWS
                     out_ref[d, 2 * i + half, :W_ROWS] = term[at : at + W_ROWS]
         begin = end
+    for copy in leaving:
+        copy.wait()
 
 
 def weight_term(target, grads, inputs):
     return call(
         weight_kernel,
-        jax.ShapeDtypeStruct((NEAR, FAR, W_ROWS + SLOT_ROWS, 2 * DH), jnp.bfloat16),
+        [
+            jax.ShapeDtypeStruct((NEAR, FAR, W_ROWS + SLOT_ROWS, 2 * DH), jnp.bfloat16),
+            jax.ShapeDtypeStruct((TOK, 2 * DH), jnp.bfloat16),
+        ],
         [target, grads, inputs],
         scratch=[
             pltpu.VMEM(inputs.shape, jnp.bfloat16),
             pltpu.VMEM((2 * DH, TOK), jnp.bfloat16),
             pltpu.VMEM((2 * DH, inputs.shape[1]), jnp.float32),
             pltpu.SemaphoreType.DMA((PER,)),
+            pltpu.SemaphoreType.DMA((PER,)),
         ],
         specs=[VMEM, VMEM, HBM],
+        out_specs=[VMEM, HBM],
         grant=WEIGHT_GRANT,
     )
 
@@ -415,10 +428,16 @@
         specs=[pl.BlockSpec(memory_space=pl.ANY)] + [VMEM] * 5,
     )
     mates = lax.ppermute(mates, "core", [(0, 1), (1, 0)])
+    slots = call(
+        slot_kernel,
+        jax.ShapeDtypeStruct((8, SLOTS), jnp.float32),
+        [picked, pairs],
+        specs=[pl.BlockSpec(memory_space=pl.ANY), VMEM],
+    )
     grads = call(
         attention_kernel,
         jax.ShapeDtypeStruct((TP, QB + ROWS, 2 * DH), bf16),
-        [bias, own, remote, kept, one, two, three, mates],
+        [slots, bias, own, remote, kept, one, two, three, mates],
         scratch=[
             pltpu.VMEM((KEYS, 2 * DH), bf16),
             pltpu.VMEM((TP, SEND, 2 * DH), bf16),
@@ -427,17 +446,12 @@
             *[pltpu.VMEM((KEYS, 2 * QB), jnp.float32)] * 4,
             *[pltpu.VMEM((KEYS, 4 * QB), bf16)] * 2,
         ],
+        specs=[pl.BlockSpec(memory_space=pl.ANY)] + [VMEM] * 8,
     )
     grads = swap(grads, tp_axes)
-    query_grad = grads[:PER, :QB].reshape(TOK, 2 * DH)
-    near = swap(weight_term(target, grads, inputs), "y")
+    near, query_grad = weight_term(target, grads, inputs)
+    near = swap(near, "y")
     far = call(regroup_kernel, jax.ShapeDtypeStruct((FAR, W_ROWS + NEAR * SLOT_ROWS, 2 * DH), bf16), [near])
-    slots = call(
-        slot_kernel,
-        jax.ShapeDtypeStruct((8, SLOTS), jnp.float32),
-        [far, pairs],
-        specs=[pl.BlockSpec(memory_space=pl.ANY), VMEM],
-    )
     far = swap(far, "z")
     keyval_grad, weight_grad = call(
         home_kernel,

time: 115 us -> 114 us (level)
  blocking collectives: 24.7 us -> 52.5 us
  waiting for transfers between devices: 26.1 us -> 8.47 us
  starting transfers between devices: 46.7 us -> 36.1 us
    all_to_all x2 -> x3, blocking collectives: 24.7 us -> 52.5 us  [swap(): return lax.all_to_all(array, axis, 0, 0, tiled=True)]
    all_to_all x3 -> x2, waiting for transfers between devices: 26.1 us -> 8.46 us  [swap(): return lax.all_to_all(array, axis, 0, 0, tiled=True)]
    all_to_all x3 -> x2, starting transfers between devices: 33.4 us -> 22.8 us  [swap(): return lax.all_to_all(array, axis, 0, 0, tiled=True)]
  transfers between devices with their start and end apart: 7 -> 6, of which waited for: 3 -> 2; matrix products, arithmetic and copies ran while one was open for 2% -> 2% of each run, Pallas kernels for 1% -> 1%
where the time goes in v3:
time: 114 us
  blocking collectives  52.5 us (46%)
  starting transfers between devices  36.1 us (32%)
  Pallas kernels  11.6 us (10%)
  waiting for transfers between devices  8.47 us (7%)
  local copies, waits for them, and re-layouts  3.84 us (3%)
    all_to_all x3, blocking collectives, swap(): return lax.all_to_all(array, axis, 0, 0, tiled=True)  52.5 us
    all_to_all x2, starting transfers between devices, swap(): return lax.all_to_all(array, axis, 0, 0, tiled=True)  22.8 us
    pallas_call x8, Pallas kernels, call(): pl.pallas_call(kernel, out_shape=out_shape, in_specs=specs or [VMEM for _...  11.6 us
    ppermute x3, starting transfers between devices, shift(): return lax.ppermute(array, 'x', [(i, (i + k) % 4) for i in range(4)])  11.4 us
    all_to_all x2, waiting for transfers between devices, swap(): return lax.all_to_all(array, axis, 0, 0, tiled=True)  8.46 us
    unnamed x7, local copies, waits for them, and re-layouts  2.59 us
  transfers between devices with their start and end apart: 6, of which 2 were waited for; matrix products, arithmetic and copies ran while one was open for 2% of the time, Pallas kernels for 1%

profile of v3, /device:TPU:32, one launch (start us, length us, event | category | flops | bytes accessed | tf_op | source)
XLA Modules:
  0.0 113.7 jit_solution(8860445856975862715)
XLA Ops:
  0.6 3.1 %shard_map.85 = (bf16[512,128]{1,0:T(8,128)(2,1)}, f32[128,128]{1,0:T(8,128)}, bf16[8,16,128]{2,1,0:T(8,128)(2,1)}, bf16[2,272,128]{2,1,0:T(8,128)(2,1)}, bf16[2...) custom-call(s32[16,448]{1,0:T(8,128)} %bitcast.8, bf16[896,128]{1,0:T(8,128)(2,1)} %kv_hbm.1, ...), custom_call_target="tpu_custom_call" | custom-call | tf_op jit(solution)/shard_map/pallas_call | solution.py:44
  3.8 18.4 %all-to-all-start = ((bf16[64,8,128]{2,1,0:T(8,128)(2,1)}), bf16[64,8,128]{2,1,0:T(8,128)(2,1)S(1)}, u32[]{:S(2)}, u32[]{:S(2)}) async-start(bf16[64,8,128]{2,1,0:T(8,128)(2,1)} %bitcast.7), calls=%async_computation | async-start | bytes 262144 | tf_op jit(solution)/shard_map/all_to_all | solution.py:362
  22.2 3.4 %collective-permute-start = (bf16[2,272,128]{2,1,0:T(8,128)(2,1)}, bf16[2,272,128]{2,1,0:T(8,128)(2,1)S(1)}, u32[]{:S(2)}, u32[]{:S(2)}) collective-permute-start(bf16[2,272,128]{2,1,0:T(8,128)(2,1)} %get-tuple-element.21), channel_id=1, source_target_pairs={{0,2},{2,4},{4,6},{6,0},{1,3},{3,5},{5,7},{7,1},{8,10},{10,12},{12... | collective-permute-start | bytes 417800 | tf_op jit(solution)/shard_map/ppermute | solution.py:397
  25.6 4.6 %collective-permute-start.1 = (bf16[2,272,128]{2,1,0:T(8,128)(2,1)}, bf16[2,272,128]{2,1,0:T(8,128)(2,1)S(1)}, u32[]{:S(2)}, u32[]{:S(2)}) collective-permute-start(bf16[2,272,128]{2,1,0:T(8,128)(2,1)} %get-tuple-element.22), channel_id=1, source_target_pairs={{0,4},{2,6},{4,0},{6,2},{1,5},{3,7},{5,1},{7,3},{8,12},{10,14},{12... | collective-permute-start | bytes 417800 | tf_op jit(solution)/shard_map/ppermute | solution.py:397
  30.2 3.3 %collective-permute-start.2 = (bf16[2,272,128]{2,1,0:T(8,128)(2,1)}, bf16[2,272,128]{2,1,0:T(8,128)(2,1)S(1)}, u32[]{:S(2)}, u32[]{:S(2)}) collective-permute-start(bf16[2,272,128]{2,1,0:T(8,128)(2,1)} %get-tuple-element.23), channel_id=1, source_target_pairs={{0,6},{2,0},{4,2},{6,4},{1,7},{3,1},{5,3},{7,5},{8,14},{10,8},{12,... | collective-permute-start | bytes 417800 | tf_op jit(solution)/shard_map/ppermute | solution.py:397
  33.6 0.8 dynamic-slice
  34.6 0.2 select_reduce_fusion
  35.0 0.1 convert_element_type.6.target_ref
  35.1 3.8 %all-to-all-done = bf16[64,8,128]{2,1,0:T(8,128)(2,1)S(1)} async-done(((bf16[64,8,128]{2,1,0:T(8,128)(2,1)}), bf16[64,8,128]{2,1,0:T(8,128)(2,1)S(1)}, u32[]{:S(2)}, u32[]{:S(2)}) %all-to-all-start) | async-done | bytes 131104 | tf_op jit(solution)/shard_map/all_to_all | solution.py:362
  38.9 1.0 shard_map.86.after_ref
  39.9 0.9 copy-done
  40.8 0.8 copy-done.2
  41.6 1.9 %collective-permute-start.3 = (bf16[4,272,128]{2,1,0:T(8,128)(2,1)S(1)}, bf16[4,272,128]{2,1,0:T(8,128)(2,1)S(1)}, u32[]{:S(2)}, u32[]{:S(2)}) collective-permute-start(bf16[4,272,128]{2,1,0:T(8,128)(2,1)S(1)} %get-tuple-element.26), channel_id=1, source_target_pairs={{0,1},{1,0},{2,3},{3,2},{4,5},{5,4},{6,7},{7,6},{8,9},{9,8},{10,11... | collective-permute-start | bytes 835592 | tf_op jit(solution)/shard_map/ppermute | solution.py:430
  43.6 4.4 %all-to-all-start.1 = ((bf16[8,48,128]{2,1,0:T(8,128)(2,1)}), bf16[8,48,128]{2,1,0:T(8,128)(2,1)S(1)}, u32[]{:S(2)}, u32[]{:S(2)}) async-start(bf16[8,48,128]{2,1,0:T(8,128)(2,1)} %shard_map.86.after_ref), calls=%async_computation.1 | async-start | bytes 196608 | tf_op jit(solution)/shard_map/all_to_all | solution.py:362
  48.1 0.1 broadcast_in_dim.54.bias_ref
  48.2 0.8 copy-done.1
  49.0 0.1 shard_map.87.after_ref.slot_ref
  49.1 4.7 %all-to-all-done.1.remote_ref = bf16[8,48,128]{2,1,0:T(8,128)(2,1)S(1)} async-done(((bf16[8,48,128]{2,1,0:T(8,128)(2,1)}), bf16[8,48,128]{2,1,0:T(8,128)(2,1)S(1)}, u32[]{:S(2)}, u32[]{:S(2)}) %all-to-all-start.1) | async-done | bytes 98336 | tf_op jit(solution)/shard_map/all_to_all | solution.py:362
  53.8 3.6 %shard_map.89 = bf16[8,192,128]{2,1,0:T(8,128)(2,1)S(1)} custom-call(f32[8,512]{1,0:T(8,128)S(1)} %shard_map.87.after_ref.slot_ref, f32[1,512]{1,0:T(1,128)S(1)} %broadcast_in_dim.54.bias_ref, bf16[8,16,128]{2,1,0:T(8,128)(2,1)S(1)} %get-tuple-element.24.own_ref, bf16[8,48,128]{2,1,0:T(8,128)(2,1)S(1)} %all-to-all-done.1.remote_ref, ...), custom_call_target="tpu_custom_call" | custom-call | tf_op jit(solution)/shard_map/pallas_call | solution.py:44
  57.4 11.3 %all_to_all.25.grad_ref.grads_ref = bf16[8,192,128]{2,1,0:T(8,128)(2,1)S(1)} all-to-all(bf16[8,192,128]{2,1,0:T(8,128)(2,1)S(1)} %shard_map.89), channel_id=1, replica_groups=mesh['z'=16,'y'=4,'x'=4,'core'=2] {'x','core'}, dimensions={0} | all-to-all | bytes 786432 | tf_op jit(solution)/shard_map/all_to_all | solution.py:362
  68.7 2.9 %shard_map.90 = (bf16[4,16,40,128]{3,2,1,0:T(8,128)(2,1)S(1)}, bf16[896,128]{1,0:T(8,128)(2,1)}) custom-call(f32[1,512]{1,0:T(1,128)S(1)} %convert_element_type.6.target_ref, bf16[8,192,128]{2,1,0:T(8,128)(2,1)S(1)} %all_to_all.25.grad_ref.grads_ref, bf16[896,2048]{1,0:T(8,128)(2,1)} %in_hbm.1), custom_call_target="tpu_custom_call" | custom-call | tf_op jit(solution)/shard_map/pallas_call | solution.py:44
  71.6 13.4 %all_to_all.26.in_ref = bf16[4,16,40,128]{3,2,1,0:T(8,128)(2,1)S(1)} all-to-all(bf16[4,16,40,128]{3,2,1,0:T(8,128)(2,1)S(1)} %get-tuple-element.28), channel_id=1, replica_groups=mesh['z'=16,'y'=4,'x'=4,'core'=2] {'y'}, dimensions={0} | all-to-all | bytes 1310720 | tf_op jit(solution)/shard_map/all_to_all | solution.py:362
  85.0 27.9 %all_to_all.27.returned_ref = bf16[16,64,128]{2,1,0:T(8,128)(2,1)S(1)} all-to-all(bf16[16,64,128]{2,1,0:T(8,128)(2,1)S(1)} %shard_map.91), channel_id=1, replica_groups=mesh['z'=16,'y'=4,'x'=4,'core'=2] {'z'}, dimensions={0} | all-to-all | bytes 524288 | tf_op jit(solution)/shard_map/all_to_all | solution.py:362
  112.9 0.8 shard_map.92
  (21 shorter events, 0.7 us)
Async XLA Ops:
  3.8 35.1 %all-to-all-start = ((bf16[64,8,128]{2,1,0:T(8,128)(2,1)}), bf16[64,8,128]{2,1,0:T(8,128)(2,1)S(1)}, u32[]{:S(2)}, u32[]{:S(2)}) async-start(bf16[64,8,128]{2,1,0:T(8,128)(2,1)} %bitcast.7), calls=%async_computation | async-start | bytes 262144 | tf_op jit(solution)/shard_map/all_to_all | solution.py:362
  22.2 17.7 %collective-permute-start = (bf16[2,272,128]{2,1,0:T(8,128)(2,1)}, bf16[2,272,128]{2,1,0:T(8,128)(2,1)S(1)}, u32[]{:S(2)}, u32[]{:S(2)}) collective-permute-start(bf16[2,272,128]{2,1,0:T(8,128)(2,1)} %get-tuple-element.21), channel_id=1, source_target_pairs={{0,2},{2,4},{4,6},{6,0},{1,3},{3,5},{5,7},{7,1},{8,10},{10,12},{12... | collective-permute-start | bytes 417800 | tf_op jit(solution)/shard_map/ppermute | solution.py:397
  25.6 14.3 %collective-permute-start.1 = (bf16[2,272,128]{2,1,0:T(8,128)(2,1)}, bf16[2,272,128]{2,1,0:T(8,128)(2,1)S(1)}, u32[]{:S(2)}, u32[]{:S(2)}) collective-permute-start(bf16[2,272,128]{2,1,0:T(8,128)(2,1)} %get-tuple-element.22), channel_id=1, source_target_pairs={{0,4},{2,6},{4,0},{6,2},{1,5},{3,7},{5,1},{7,3},{8,12},{10,14},{12... | collective-permute-start | bytes 417800 | tf_op jit(solution)/shard_map/ppermute | solution.py:397
  30.2 9.7 %collective-permute-start.2 = (bf16[2,272,128]{2,1,0:T(8,128)(2,1)}, bf16[2,272,128]{2,1,0:T(8,128)(2,1)S(1)}, u32[]{:S(2)}, u32[]{:S(2)}) collective-permute-start(bf16[2,272,128]{2,1,0:T(8,128)(2,1)} %get-tuple-element.23), channel_id=1, source_target_pairs={{0,6},{2,0},{4,2},{6,4},{1,7},{3,1},{5,3},{7,5},{8,14},{10,8},{12,... | collective-permute-start | bytes 417800 | tf_op jit(solution)/shard_map/ppermute | solution.py:397
  39.9 0.9 copy-start
  40.8 0.8 copy-start.2
  41.6 12.2 %collective-permute-start.3 = (bf16[4,272,128]{2,1,0:T(8,128)(2,1)S(1)}, bf16[4,272,128]{2,1,0:T(8,128)(2,1)S(1)}, u32[]{:S(2)}, u32[]{:S(2)}) collective-permute-start(bf16[4,272,128]{2,1,0:T(8,128)(2,1)S(1)} %get-tuple-element.26), channel_id=1, source_target_pairs={{0,1},{1,0},{2,3},{3,2},{4,5},{5,4},{6,7},{7,6},{8,9},{9,8},{10,11... | collective-permute-start | bytes 835592 | tf_op jit(solution)/shard_map/ppermute | solution.py:430
  43.6 10.2 %all-to-all-start.1 = ((bf16[8,48,128]{2,1,0:T(8,128)(2,1)}), bf16[8,48,128]{2,1,0:T(8,128)(2,1)S(1)}, u32[]{:S(2)}, u32[]{:S(2)}) async-start(bf16[8,48,128]{2,1,0:T(8,128)(2,1)} %shard_map.86.after_ref), calls=%async_computation.1 | async-start | bytes 196608 | tf_op jit(solution)/shard_map/all_to_all | solution.py:362
  48.2 0.8 copy-start.1

commit v4 on v3

--- a/solution.py
+++ b/solution.py
@@ -109,15 +109,6 @@
     other = lax.broadcasted_iota(jnp.int32, (KV, 128), 0) != me
     pair_ref[:KV] = jnp.where(other & (least < OWN), least, -1000.0)
     pair_ref[KV:] = jnp.where(other, most, -1000.0)
-    gets[1].wait()
-    piece = jnp.dot(mine, kv_ref[...], preferred_element_type=jnp.float32).astype(jnp.bfloat16)
-    at = lax.broadcasted_iota(jnp.int32, (SLOT_ROWS, 128), 1) - (
-        lax.broadcasted_iota(jnp.int32, (SLOT_ROWS, 128), 0) & (PIECE - 1)
-    )
-    at = jnp.where((at & (PIECE - 1)) == 0, at >> 2, -1).astype(jnp.float32)
-    onehot = slot_blocks(pair_ref).reshape(KV, SLOT_ROWS, 128) == at[None]
-    onehot = onehot.reshape(SLOTS, 128).astype(jnp.bfloat16)
-    out_ref[...] = jnp.dot(onehot, piece, preferred_element_type=jnp.float32).astype(jnp.bfloat16)
     gets[2].wait()
     gets[3].wait()
     gets[4].wait()
@@ -140,17 +131,27 @@
             pltpu.make_async_copy(term_ref.at[:, pl.ds(at, QB)], to.at[pl.ds(LOG_AT, 16)], own_sems.at[j, 2])
         )
         copies[-1].start()
+    gets[1].wait()
     row = lax.broadcasted_iota(jnp.int32, (QB, QB), 0)
     turn = ((row >> 2) & 3) * KB + (row >> 4) * PIECE + (row & (PIECE - 1))
     turn = (turn == lax.broadcasted_iota(jnp.int32, (QB, QB), 1)).astype(jnp.bfloat16)
     own_at = pl.multiple_of(jnp.minimum(member, PER - 1) * QB, QB)
     own = jnp.dot(turn, kv_ref[pl.ds(own_at, QB)], preferred_element_type=jnp.float32)
     own_ref[...] = own.astype(jnp.bfloat16).reshape(TP, DIAG * PIECE, 2 * DH)
+    piece = jnp.dot(mine, kv_ref[...], preferred_element_type=jnp.float32).astype(jnp.bfloat16)
+    at = lax.broadcasted_iota(jnp.int32, (SLOT_ROWS, 128), 1) - (
+        lax.broadcasted_iota(jnp.int32, (SLOT_ROWS, 128), 0) & (PIECE - 1)
+    )
+    at = jnp.where((at & (PIECE - 1)) == 0, at >> 2, -1).astype(jnp.float32)
+    onehot = slot_blocks(pair_ref).reshape(KV, SLOT_ROWS, 128) == at[None]
+    onehot = onehot.reshape(SLOTS, 128).astype(jnp.bfloat16)
+    out_ref[...] = jnp.dot(onehot, piece, preferred_element_type=jnp.float32).astype(jnp.bfloat16)
     for copy in copies:
         copy.wait()
 
 
-def slot_kernel(after_ref, pair_ref, slot_ref):
+def slot_kernel(after_ref, pair_ref, given_ref, slot_ref, own_ref):
+    own_ref[...] = given_ref[...]
     piece_row = lax.broadcasted_iota(jnp.int32, (SLOTS, 128), 0) & (PIECE - 1)
     home = slot_blocks(pair_ref) * PIECE + piece_row.astype(jnp.float32)
     slot_ref[...] = home.T[:8]
@@ -168,9 +169,8 @@
         out_ref[t] = rows[t * ROWS : t * ROWS + REM_ROWS]
 
 
-def mate_kernel(after_ref, given_ref, zero_ref, one_ref, two_ref, three_ref, out_ref, kept_ref, own_ref):
+def mate_kernel(after_ref, zero_ref, one_ref, two_ref, three_ref, out_ref, kept_ref):
     kept_ref[...] = zero_ref[0]
-    own_ref[...] = given_ref[...]
     for k, ref in enumerate((zero_ref, one_ref, two_ref, three_ref)):
         out_ref[k] = ref[1]
 
@@ -417,22 +417,22 @@
         pick_kernel, jax.ShapeDtypeStruct((TP, REM_ROWS, 2 * DH), bf16), [target, fetched.reshape(SLOTS, 2 * DH)]
     )
     remote = swap(picked, tp_axes)
-    mates, kept, own = call(
+    mates, kept = call(
         mate_kernel,
+        [jax.ShapeDtypeStruct((4, SEND, 2 * DH), bf16), jax.ShapeDtypeStruct((SEND, 2 * DH), bf16)],
+        [picked, blocks[0], one, two, three],
+        specs=[pl.BlockSpec(memory_space=pl.ANY)] + [VMEM] * 4,
+    )
+    given = mates
+    mates = lax.ppermute(mates, "core", [(0, 1), (1, 0)])
+    slots, own = call(
+        slot_kernel,
         [
-            jax.ShapeDtypeStruct((4, SEND, 2 * DH), bf16),
-            jax.ShapeDtypeStruct((SEND, 2 * DH), bf16),
+            jax.ShapeDtypeStruct((8, SLOTS), jnp.float32),
             jax.ShapeDtypeStruct((TP, DIAG * PIECE, 2 * DH), bf16),
         ],
-        [picked, own, blocks[0], one, two, three],
-        specs=[pl.BlockSpec(memory_space=pl.ANY)] + [VMEM] * 5,
-    )
-    mates = lax.ppermute(mates, "core", [(0, 1), (1, 0)])
-    slots = call(
-        slot_kernel,
-        jax.ShapeDtypeStruct((8, SLOTS), jnp.float32),
-        [picked, pairs],
-        specs=[pl.BlockSpec(memory_space=pl.ANY), VMEM],
+        [given, pairs, own],
+        specs=[pl.BlockSpec(memory_space=pl.ANY), VMEM, VMEM],
     )
     grads = call(
         attention_kernel,

time: 114 us -> 113 us (level)
  no operation moved by 1% of the time
where the time goes in v4:
time: 113 us
  blocking collectives  52.5 us (46%)
  starting transfers between devices  36.1 us (32%)
  Pallas kernels  11.4 us (10%)
  waiting for transfers between devices  7.71 us (7%)
  local copies, waits for them, and re-layouts  3.84 us (3%)
    all_to_all x3, blocking collectives, swap(): return lax.all_to_all(array, axis, 0, 0, tiled=True)  52.5 us
    all_to_all x2, starting transfers between devices, swap(): return lax.all_to_all(array, axis, 0, 0, tiled=True)  22.8 us
    ppermute x3, starting transfers between devices, shift(): return lax.ppermute(array, 'x', [(i, (i + k) % 4) for i in range(4)])  11.4 us
    pallas_call x8, Pallas kernels, call(): pl.pallas_call(kernel, out_shape=out_shape, in_specs=specs or [VMEM for _...  11.4 us
    all_to_all x2, waiting for transfers between devices, swap(): return lax.all_to_all(array, axis, 0, 0, tiled=True)  7.7 us
    unnamed x7, local copies, waits for them, and re-layouts  2.59 us
  transfers between devices with their start and end apart: 6, of which 2 were waited for; matrix products, arithmetic and copies ran while one was open for 2% of the time, Pallas kernels for 1%

profile of v4, /device:TPU:32, one launch (start us, length us, event | category | flops | bytes accessed | tf_op | source)
XLA Modules:
  0.0 112.7 jit_solution(10894907915344641392)
XLA Ops:
  0.6 2.9 %shard_map.85 = (bf16[512,128]{1,0:T(8,128)(2,1)}, f32[128,128]{1,0:T(8,128)}, bf16[8,16,128]{2,1,0:T(8,128)(2,1)}, bf16[2,272,128]{2,1,0:T(8,128)(2,1)}, bf16[2...) custom-call(s32[16,448]{1,0:T(8,128)} %bitcast.8, bf16[896,128]{1,0:T(8,128)(2,1)} %kv_hbm.1, ...), custom_call_target="tpu_custom_call" | custom-call | tf_op jit(solution)/shard_map/pallas_call | solution.py:44
  3.6 18.4 %all-to-all-start = ((bf16[64,8,128]{2,1,0:T(8,128)(2,1)}), bf16[64,8,128]{2,1,0:T(8,128)(2,1)S(1)}, u32[]{:S(2)}, u32[]{:S(2)}) async-start(bf16[64,8,128]{2,1,0:T(8,128)(2,1)} %bitcast.7), calls=%async_computation | async-start | bytes 262144 | tf_op jit(solution)/shard_map/all_to_all | solution.py:362
  22.0 3.4 %collective-permute-start = (bf16[2,272,128]{2,1,0:T(8,128)(2,1)}, bf16[2,272,128]{2,1,0:T(8,128)(2,1)S(1)}, u32[]{:S(2)}, u32[]{:S(2)}) collective-permute-start(bf16[2,272,128]{2,1,0:T(8,128)(2,1)} %get-tuple-element.20), channel_id=1, source_target_pairs={{0,2},{2,4},{4,6},{6,0},{1,3},{3,5},{5,7},{7,1},{8,10},{10,12},{12... | collective-permute-start | bytes 417800 | tf_op jit(solution)/shard_map/ppermute | solution.py:397
  25.4 4.6 %collective-permute-start.1 = (bf16[2,272,128]{2,1,0:T(8,128)(2,1)}, bf16[2,272,128]{2,1,0:T(8,128)(2,1)S(1)}, u32[]{:S(2)}, u32[]{:S(2)}) collective-permute-start(bf16[2,272,128]{2,1,0:T(8,128)(2,1)} %get-tuple-element.21), channel_id=1, source_target_pairs={{0,4},{2,6},{4,0},{6,2},{1,5},{3,7},{5,1},{7,3},{8,12},{10,14},{12... | collective-permute-start | bytes 417800 | tf_op jit(solution)/shard_map/ppermute | solution.py:397
  30.0 3.3 %collective-permute-start.2 = (bf16[2,272,128]{2,1,0:T(8,128)(2,1)}, bf16[2,272,128]{2,1,0:T(8,128)(2,1)S(1)}, u32[]{:S(2)}, u32[]{:S(2)}) collective-permute-start(bf16[2,272,128]{2,1,0:T(8,128)(2,1)} %get-tuple-element.22), channel_id=1, source_target_pairs={{0,6},{2,0},{4,2},{6,4},{1,7},{3,1},{5,3},{7,5},{8,14},{10,8},{12,... | collective-permute-start | bytes 417800 | tf_op jit(solution)/shard_map/ppermute | solution.py:397
  33.4 0.8 dynamic-slice
  34.4 0.2 select_reduce_fusion
  34.8 0.1 convert_element_type.6.target_ref
  34.9 3.8 %all-to-all-done = bf16[64,8,128]{2,1,0:T(8,128)(2,1)S(1)} async-done(((bf16[64,8,128]{2,1,0:T(8,128)(2,1)}), bf16[64,8,128]{2,1,0:T(8,128)(2,1)S(1)}, u32[]{:S(2)}, u32[]{:S(2)}) %all-to-all-start) | async-done | bytes 131104 | tf_op jit(solution)/shard_map/all_to_all | solution.py:362
  38.7 1.0 shard_map.86.after_ref
  39.7 0.9 copy-done
  40.6 1.9 %collective-permute-start.3 = (bf16[4,272,128]{2,1,0:T(8,128)(2,1)S(1)}, bf16[4,272,128]{2,1,0:T(8,128)(2,1)S(1)}, u32[]{:S(2)}, u32[]{:S(2)}) collective-permute-start(bf16[4,272,128]{2,1,0:T(8,128)(2,1)S(1)} %get-tuple-element.23.after_ref), channel_id=1, source_target_pairs={{0,1},{1,0},{2,3},{3,2},{4,5},{5,4},{6,7},{7,6},{8,9},{9,8},{10,11... | collective-permute-start | bytes 835592 | tf_op jit(solution)/shard_map/ppermute | solution.py:427
  42.6 4.4 %all-to-all-start.1 = ((bf16[8,48,128]{2,1,0:T(8,128)(2,1)}), bf16[8,48,128]{2,1,0:T(8,128)(2,1)S(1)}, u32[]{:S(2)}, u32[]{:S(2)}) async-start(bf16[8,48,128]{2,1,0:T(8,128)(2,1)} %shard_map.86.after_ref), calls=%async_computation.1 | async-start | bytes 196608 | tf_op jit(solution)/shard_map/all_to_all | solution.py:362
  47.1 0.1 broadcast_in_dim.54.bias_ref
  47.2 0.8 copy-done.1
  48.1 0.8 copy-done.2
  48.8 0.1 shard_map.88
  48.9 3.9 %all-to-all-done.1.remote_ref = bf16[8,48,128]{2,1,0:T(8,128)(2,1)S(1)} async-done(((bf16[8,48,128]{2,1,0:T(8,128)(2,1)}), bf16[8,48,128]{2,1,0:T(8,128)(2,1)S(1)}, u32[]{:S(2)}, u32[]{:S(2)}) %all-to-all-start.1) | async-done | bytes 98336 | tf_op jit(solution)/shard_map/all_to_all | solution.py:362
  52.8 3.6 %shard_map.89 = bf16[8,192,128]{2,1,0:T(8,128)(2,1)S(1)} custom-call(f32[8,512]{1,0:T(8,128)S(1)} %get-tuple-element.26.after_ref.slot_ref, f32[1,512]{1,0:T(1,128)S(1)} %broadcast_in_dim.54.bias_ref, bf16[8,16,128]{2,1,0:T(8,128)(2,1)S(1)} %get-tuple-element.27.own_ref, bf16[8,48,128]{2,1,0:T(8,128)(2,1)S(1)} %all-to-all-done.1.remote_ref, ...), custom_call_target="tpu_custom_call" | custom-call | tf_op jit(solution)/shard_map/pallas_call | solution.py:44
  56.4 11.3 %all_to_all.25.grad_ref.grads_ref = bf16[8,192,128]{2,1,0:T(8,128)(2,1)S(1)} all-to-all(bf16[8,192,128]{2,1,0:T(8,128)(2,1)S(1)} %shard_map.89), channel_id=1, replica_groups=mesh['z'=16,'y'=4,'x'=4,'core'=2] {'x','core'}, dimensions={0} | all-to-all | bytes 786432 | tf_op jit(solution)/shard_map/all_to_all | solution.py:362
  67.7 2.9 %shard_map.90 = (bf16[4,16,40,128]{3,2,1,0:T(8,128)(2,1)S(1)}, bf16[896,128]{1,0:T(8,128)(2,1)}) custom-call(f32[1,512]{1,0:T(1,128)S(1)} %convert_element_type.6.target_ref, bf16[8,192,128]{2,1,0:T(8,128)(2,1)S(1)} %all_to_all.25.grad_ref.grads_ref, bf16[896,2048]{1,0:T(8,128)(2,1)} %in_hbm.1), custom_call_target="tpu_custom_call" | custom-call | tf_op jit(solution)/shard_map/pallas_call | solution.py:44
  70.6 13.4 %all_to_all.26.in_ref = bf16[4,16,40,128]{3,2,1,0:T(8,128)(2,1)S(1)} all-to-all(bf16[4,16,40,128]{3,2,1,0:T(8,128)(2,1)S(1)} %get-tuple-element.30), channel_id=1, replica_groups=mesh['z'=16,'y'=4,'x'=4,'core'=2] {'y'}, dimensions={0} | all-to-all | bytes 1310720 | tf_op jit(solution)/shard_map/all_to_all | solution.py:362
  84.1 27.8 %all_to_all.27.returned_ref = bf16[16,64,128]{2,1,0:T(8,128)(2,1)S(1)} all-to-all(bf16[16,64,128]{2,1,0:T(8,128)(2,1)S(1)} %shard_map.91), channel_id=1, replica_groups=mesh['z'=16,'y'=4,'x'=4,'core'=2] {'z'}, dimensions={0} | all-to-all | bytes 524288 | tf_op jit(solution)/shard_map/all_to_all | solution.py:362
  111.9 0.8 shard_map.92
  (21 shorter events, 0.6 us)
Async XLA Ops:
  3.6 35.1 %all-to-all-start = ((bf16[64,8,128]{2,1,0:T(8,128)(2,1)}), bf16[64,8,128]{2,1,0:T(8,128)(2,1)S(1)}, u32[]{:S(2)}, u32[]{:S(2)}) async-start(bf16[64,8,128]{2,1,0:T(8,128)(2,1)} %bitcast.7), calls=%async_computation | async-start | bytes 262144 | tf_op jit(solution)/shard_map/all_to_all | solution.py:362
  22.0 17.7 %collective-permute-start = (bf16[2,272,128]{2,1,0:T(8,128)(2,1)}, bf16[2,272,128]{2,1,0:T(8,128)(2,1)S(1)}, u32[]{:S(2)}, u32[]{:S(2)}) collective-permute-start(bf16[2,272,128]{2,1,0:T(8,128)(2,1)} %get-tuple-element.20), channel_id=1, source_target_pairs={{0,2},{2,4},{4,6},{6,0},{1,3},{3,5},{5,7},{7,1},{8,10},{10,12},{12... | collective-permute-start | bytes 417800 | tf_op jit(solution)/shard_map/ppermute | solution.py:397
  25.4 14.3 %collective-permute-start.1 = (bf16[2,272,128]{2,1,0:T(8,128)(2,1)}, bf16[2,272,128]{2,1,0:T(8,128)(2,1)S(1)}, u32[]{:S(2)}, u32[]{:S(2)}) collective-permute-start(bf16[2,272,128]{2,1,0:T(8,128)(2,1)} %get-tuple-element.21), channel_id=1, source_target_pairs={{0,4},{2,6},{4,0},{6,2},{1,5},{3,7},{5,1},{7,3},{8,12},{10,14},{12... | collective-permute-start | bytes 417800 | tf_op jit(solution)/shard_map/ppermute | solution.py:397
  30.0 9.7 %collective-permute-start.2 = (bf16[2,272,128]{2,1,0:T(8,128)(2,1)}, bf16[2,272,128]{2,1,0:T(8,128)(2,1)S(1)}, u32[]{:S(2)}, u32[]{:S(2)}) collective-permute-start(bf16[2,272,128]{2,1,0:T(8,128)(2,1)} %get-tuple-element.22), channel_id=1, source_target_pairs={{0,6},{2,0},{4,2},{6,4},{1,7},{3,1},{5,3},{7,5},{8,14},{10,8},{12,... | collective-permute-start | bytes 417800 | tf_op jit(solution)/shard_map/ppermute | solution.py:397
  39.7 0.9 copy-start
  40.6 12.2 %collective-permute-start.3 = (bf16[4,272,128]{2,1,0:T(8,128)(2,1)S(1)}, bf16[4,272,128]{2,1,0:T(8,128)(2,1)S(1)}, u32[]{:S(2)}, u32[]{:S(2)}) collective-permute-start(bf16[4,272,128]{2,1,0:T(8,128)(2,1)S(1)} %get-tuple-element.23.after_ref), channel_id=1, source_target_pairs={{0,1},{1,0},{2,3},{3,2},{4,5},{5,4},{6,7},{7,6},{8,9},{9,8},{10,11... | collective-permute-start | bytes 835592 | tf_op jit(solution)/shard_map/ppermute | solution.py:427
  42.6 10.2 %all-to-all-start.1 = ((bf16[8,48,128]{2,1,0:T(8,128)(2,1)}), bf16[8,48,128]{2,1,0:T(8,128)(2,1)S(1)}, u32[]{:S(2)}, u32[]{:S(2)}) async-start(bf16[8,48,128]{2,1,0:T(8,128)(2,1)} %shard_map.86.after_ref), calls=%async_computation.1 | async-start | bytes 196608 | tf_op jit(solution)/shard_map/all_to_all | solution.py:362
  47.2 0.8 copy-start.1
  48.1 0.8 copy-start.2

commit v5 on v4

--- a/solution.py
+++ b/solution.py
@@ -29,6 +29,7 @@
 LOG_AT = 2 * QB
 SEND = LOG_AT + 16
 SLOT_ROWS = CAP * PIECE
+TAIL_AT = 2 * SEND
 W_ROWS = 32
 NEAR, FAR = 4, 16
 LOG2E = 1.4426950408889634
@@ -73,9 +74,10 @@
 
 
 def offer_kernel(
-    sel_hbm, kv_hbm, q_hbm, g_hbm, log_hbm, out_ref, pair_ref, own_ref, *refs
+    sel_hbm, kv_hbm, q_hbm, g_hbm, log_hbm, out_ref, near_hbm, *refs
 ):
-    block_refs, (sel_ref, kv_ref, q_ref, g_ref, log_ref, term_ref, sems, own_sems) = refs[:4], refs[4:]
+    block_refs = refs[:3]
+    sel_ref, kv_ref, q_ref, g_ref, log_ref, term_ref, pair_ref, tail_ref, sems, own_sems = refs[3:]
     gets = [
         pltpu.make_async_copy(hbm, ref, sems.at[i])
         for i, (hbm, ref) in enumerate(
@@ -89,7 +91,8 @@
     for k in range(4):
         for j, side in enumerate((core, 1 - core)):
             block = ((x + k) & 3) * 2 + side
-            places.append((block_refs[k].at[j], pl.multiple_of(jnp.minimum(block, PER - 1) * QB, QB)))
+            to = block_refs[k - 1].at[j] if k else near_hbm.at[pl.ds(j * SEND, SEND)]
+            places.append((to, pl.multiple_of(jnp.minimum(block, PER - 1) * QB, QB)))
     me, member = kv_index(), member_index()
     row = lax.broadcasted_iota(jnp.int32, (128, TOK), 0)
     col = lax.broadcasted_iota(jnp.int32, (128, TOK), 1)
@@ -137,7 +140,10 @@
     turn = (turn == lax.broadcasted_iota(jnp.int32, (QB, QB), 1)).astype(jnp.bfloat16)
     own_at = pl.multiple_of(jnp.minimum(member, PER - 1) * QB, QB)
     own = jnp.dot(turn, kv_ref[pl.ds(own_at, QB)], preferred_element_type=jnp.float32)
-    own_ref[...] = own.astype(jnp.bfloat16).reshape(TP, DIAG * PIECE, 2 * DH)
+    tail_ref[:QB] = own.astype(jnp.bfloat16)
+    tail_ref[QB:] = pair_ref[...].astype(jnp.bfloat16)
+    copies.append(pltpu.make_async_copy(tail_ref, near_hbm.at[pl.ds(TAIL_AT, 2 * QB)], sems.at[5]))
+    copies[-1].start()
     piece = jnp.dot(mine, kv_ref[...], preferred_element_type=jnp.float32).astype(jnp.bfloat16)
     at = lax.broadcasted_iota(jnp.int32, (SLOT_ROWS, 128), 1) - (
         lax.broadcasted_iota(jnp.int32, (SLOT_ROWS, 128), 0) & (PIECE - 1)
@@ -150,8 +156,8 @@
         copy.wait()
 
 
-def slot_kernel(after_ref, pair_ref, given_ref, slot_ref, own_ref):
-    own_ref[...] = given_ref[...]
+def slot_kernel(given_ref, slot_ref, pair_ref):
+    pair_ref[...] = given_ref[...].astype(jnp.float32)
     piece_row = lax.broadcasted_iota(jnp.int32, (SLOTS, 128), 0) & (PIECE - 1)
     home = slot_blocks(pair_ref) * PIECE + piece_row.astype(jnp.float32)
     slot_ref[...] = home.T[:8]
@@ -169,10 +175,13 @@
         out_ref[t] = rows[t * ROWS : t * ROWS + REM_ROWS]
 
 
-def mate_kernel(after_ref, zero_ref, one_ref, two_ref, three_ref, out_ref, kept_ref):
-    kept_ref[...] = zero_ref[0]
-    for k, ref in enumerate((zero_ref, one_ref, two_ref, three_ref)):
-        out_ref[k] = ref[1]
+def mate_kernel(after_ref, near_ref, one_ref, two_ref, three_ref, out_ref, kept_ref, own_ref, pair_ref):
+    out_ref[0] = near_ref[SEND:TAIL_AT]
+    for k, ref in enumerate((one_ref, two_ref, three_ref)):
+        out_ref[k + 1] = ref[1]
+    kept_ref[...] = near_ref[:SEND]
+    own_ref[...] = near_ref[TAIL_AT : TAIL_AT + QB].reshape(TP, DIAG * PIECE, 2 * DH)
+    pair_ref[...] = near_ref[TAIL_AT + QB :]
 
 
 def attention_kernel(
@@ -368,13 +377,13 @@
     member = member_index()
     bf16 = jnp.bfloat16
 
-    offer, pairs, own, *blocks = call(
+    block = jax.ShapeDtypeStruct((2, SEND, 2 * DH), bf16)
+    offer, nearest, *blocks = call(
         offer_kernel,
         [
             jax.ShapeDtypeStruct((SLOTS, 2 * DH), bf16),
-            jax.ShapeDtypeStruct((2 * KV, 128), jnp.float32),
-            jax.ShapeDtypeStruct((TP, DIAG * PIECE, 2 * DH), bf16),
-            *[jax.ShapeDtypeStruct((2, SEND, 2 * DH), bf16)] * 4,
+            jax.ShapeDtypeStruct((TAIL_AT + 2 * QB, 2 * DH), bf16),
+            *[block] * 3,
         ],
         [selection.T, keyvals, queries, out_grad, log_sums],
         scratch=[
@@ -384,11 +393,13 @@
             pltpu.VMEM((TOK, 2 * DH), bf16),
             pltpu.VMEM((2, TOK), jnp.float32),
             pltpu.VMEM((16, TOK), bf16),
-            pltpu.SemaphoreType.DMA((5,)),
+            pltpu.VMEM((2 * KV, 128), jnp.float32),
+            pltpu.VMEM((2 * QB, 2 * DH), bf16),
+            pltpu.SemaphoreType.DMA((6,)),
             pltpu.SemaphoreType.DMA((TP, 3)),
         ],
         specs=[HBM] * 5,
-        out_specs=[VMEM] * 3 + [HBM] * 4,
+        out_specs=[VMEM] + [HBM] * 4,
         grant=ALL_VMEM,
     )
     fetched = swap(offer.reshape(KV, SLOT_ROWS, 2 * DH), kv_axes)
@@ -396,7 +407,7 @@
     def shift(array, k):
         return lax.ppermute(array, "x", [(i, (i + k) % 4) for i in range(4)])
 
-    two, one, three = shift(blocks[2], 2), shift(blocks[1], 1), shift(blocks[3], 3)
+    two, one, three = shift(blocks[1], 2), shift(blocks[0], 1), shift(blocks[2], 3)
 
     mine = lax.dynamic_slice(selection, (me * PER, 0), (PER, NSEL))[:, DIAG:]
     flat = mine.reshape(-1)
@@ -417,22 +428,23 @@
         pick_kernel, jax.ShapeDtypeStruct((TP, REM_ROWS, 2 * DH), bf16), [target, fetched.reshape(SLOTS, 2 * DH)]
     )
     remote = swap(picked, tp_axes)
-    mates, kept = call(
+    mates, kept, own, pairs = call(
         mate_kernel,
-        [jax.ShapeDtypeStruct((4, SEND, 2 * DH), bf16), jax.ShapeDtypeStruct((SEND, 2 * DH), bf16)],
-        [picked, blocks[0], one, two, three],
+        [
+            jax.ShapeDtypeStruct((4, SEND, 2 * DH), bf16),
+            jax.ShapeDtypeStruct((SEND, 2 * DH), bf16),
+            jax.ShapeDtypeStruct((TP, DIAG * PIECE, 2 * DH), bf16),
+            jax.ShapeDtypeStruct((2 * KV, 128), bf16),
+        ],
+        [picked, nearest, one, two, three],
         specs=[pl.BlockSpec(memory_space=pl.ANY)] + [VMEM] * 4,
     )
-    given = mates
     mates = lax.ppermute(mates, "core", [(0, 1), (1, 0)])
-    slots, own = call(
+    slots = call(
         slot_kernel,
-        [
-            jax.ShapeDtypeStruct((8, SLOTS), jnp.float32),
-            jax.ShapeDtypeStruct((TP, DIAG * PIECE, 2 * DH), bf16),
-        ],
-        [given, pairs, own],
-        specs=[pl.BlockSpec(memory_space=pl.ANY), VMEM, VMEM],
+        jax.ShapeDtypeStruct((8, SLOTS), jnp.float32),
+        [pairs],
+        scratch=[pltpu.VMEM((2 * KV, 128), jnp.float32)],
     )
     grads = call(
         attention_kernel,

time: 113 us -> 113 us (level)
  waiting for transfers between devices: 7.71 us -> 9.31 us
  local copies, waits for them, and re-layouts: 3.84 us -> 2.27 us
    all_to_all x2, waiting for transfers between devices: 7.7 us -> 9.3 us  [swap(): return lax.all_to_all(array, axis, 0, 0, tiled=True)]
    unnamed x7 -> x3, local copies, waits for them, and re-layouts: 2.59 us -> 1.02 us
where the time goes in v5:
time: 113 us
  blocking collectives  52.5 us (46%)
  starting transfers between devices  36.1 us (32%)
  Pallas kernels  11.5 us (10%)
  waiting for transfers between devices  9.31 us (8%)
  local copies, waits for them, and re-layouts  2.27 us (2%)
    all_to_all x3, blocking collectives, swap(): return lax.all_to_all(array, axis, 0, 0, tiled=True)  52.5 us
    all_to_all x2, starting transfers between devices, swap(): return lax.all_to_all(array, axis, 0, 0, tiled=True)  22.8 us
    pallas_call x8, Pallas kernels, call(): pl.pallas_call(kernel, out_shape=out_shape, in_specs=specs or [VMEM for _...  11.5 us
    ppermute x3, starting transfers between devices, shift(): return lax.ppermute(array, 'x', [(i, (i + k) % 4) for i in range(4)])  11.4 us
    all_to_all x2, waiting for transfers between devices, swap(): return lax.all_to_all(array, axis, 0, 0, tiled=True)  9.3 us
  transfers between devices with their start and end apart: 6, of which 2 were waited for; matrix products, arithmetic and copies ran while one was open for 2% of the time, Pallas kernels for 1%

profile of v5, /device:TPU:32, one launch (start us, length us, event | category | flops | bytes accessed | tf_op | source)
XLA Modules:
  0.0 112.9 jit_solution(5985610887425794544)
XLA Ops:
  0.6 3.1 %shard_map.85 = (bf16[512,128]{1,0:T(8,128)(2,1)}, bf16[800,128]{1,0:T(8,128)(2,1)}, bf16[2,272,128]{2,1,0:T(8,128)(2,1)}, bf16[2,272,128]{2,1,0:T(8,128)(2,1)}, bf16[2,272,128]{2,1,0:T(8,128)(2,1)}) custom-call(s32[16,448]{1,0:T(8,128)} %bitcast.8, bf16[896,128]{1,0:T(8,128)(2,1)} %kv_hbm.1, bf16[896,128]{1,0:T(8,128)(2,1)} %q_hbm.1, ...), custom_call_target="tpu_custom_call" | custom-call | tf_op jit(solution)/shard_map/pallas_call | solution.py:45
  3.7 18.4 %all-to-all-start = ((bf16[64,8,128]{2,1,0:T(8,128)(2,1)}), bf16[64,8,128]{2,1,0:T(8,128)(2,1)S(1)}, u32[]{:S(2)}, u32[]{:S(2)}) async-start(bf16[64,8,128]{2,1,0:T(8,128)(2,1)} %bitcast.7), calls=%async_computation | async-start | bytes 262144 | tf_op jit(solution)/shard_map/all_to_all | solution.py:371
  22.1 3.4 %collective-permute-start = (bf16[2,272,128]{2,1,0:T(8,128)(2,1)}, bf16[2,272,128]{2,1,0:T(8,128)(2,1)S(1)}, u32[]{:S(2)}, u32[]{:S(2)}) collective-permute-start(bf16[2,272,128]{2,1,0:T(8,128)(2,1)} %get-tuple-element.18), channel_id=1, source_target_pairs={{0,2},{2,4},{4,6},{6,0},{1,3},{3,5},{5,7},{7,1},{8,10},{10,12},{12... | collective-permute-start | bytes 417800 | tf_op jit(solution)/shard_map/ppermute | solution.py:408
  25.5 4.6 %collective-permute-start.1 = (bf16[2,272,128]{2,1,0:T(8,128)(2,1)}, bf16[2,272,128]{2,1,0:T(8,128)(2,1)S(1)}, u32[]{:S(2)}, u32[]{:S(2)}) collective-permute-start(bf16[2,272,128]{2,1,0:T(8,128)(2,1)} %get-tuple-element.19), channel_id=1, source_target_pairs={{0,4},{2,6},{4,0},{6,2},{1,5},{3,7},{5,1},{7,3},{8,12},{10,14},{12... | collective-permute-start | bytes 417800 | tf_op jit(solution)/shard_map/ppermute | solution.py:408
  30.2 3.3 %collective-permute-start.2 = (bf16[2,272,128]{2,1,0:T(8,128)(2,1)}, bf16[2,272,128]{2,1,0:T(8,128)(2,1)S(1)}, u32[]{:S(2)}, u32[]{:S(2)}) collective-permute-start(bf16[2,272,128]{2,1,0:T(8,128)(2,1)} %get-tuple-element.20), channel_id=1, source_target_pairs={{0,6},{2,0},{4,2},{6,4},{1,7},{3,1},{5,3},{7,5},{8,14},{10,8},{12,... | collective-permute-start | bytes 417800 | tf_op jit(solution)/shard_map/ppermute | solution.py:408
  33.5 0.8 dynamic-slice
  34.3 0.1 copy.13
  34.4 0.1 reshape.102
  34.5 0.2 select_reduce_fusion
  35.0 0.1 convert_element_type.6.target_ref
  35.1 3.8 %all-to-all-done = bf16[64,8,128]{2,1,0:T(8,128)(2,1)S(1)} async-done(((bf16[64,8,128]{2,1,0:T(8,128)(2,1)}), bf16[64,8,128]{2,1,0:T(8,128)(2,1)S(1)}, u32[]{:S(2)}, u32[]{:S(2)}) %all-to-all-start) | async-done | bytes 131104 | tf_op jit(solution)/shard_map/all_to_all | solution.py:371
  38.9 1.0 shard_map.86.after_ref
  39.9 0.9 copy-done
  40.8 1.9 %collective-permute-start.3 = (bf16[4,272,128]{2,1,0:T(8,128)(2,1)S(1)}, bf16[4,272,128]{2,1,0:T(8,128)(2,1)S(1)}, u32[]{:S(2)}, u32[]{:S(2)}) collective-permute-start(bf16[4,272,128]{2,1,0:T(8,128)(2,1)S(1)} %get-tuple-element.24), channel_id=1, source_target_pairs={{0,1},{1,0},{2,3},{3,2},{4,5},{5,4},{6,7},{7,6},{8,9},{9,8},{10,11... | collective-permute-start | bytes 835592 | tf_op jit(solution)/shard_map/ppermute | solution.py:442
  42.8 4.4 %all-to-all-start.1 = ((bf16[8,48,128]{2,1,0:T(8,128)(2,1)}), bf16[8,48,128]{2,1,0:T(8,128)(2,1)S(1)}, u32[]{:S(2)}, u32[]{:S(2)}) async-start(bf16[8,48,128]{2,1,0:T(8,128)(2,1)} %shard_map.86.after_ref), calls=%async_computation.1 | async-start | bytes 196608 | tf_op jit(solution)/shard_map/all_to_all | solution.py:371
  47.3 0.1 broadcast_in_dim.54.bias_ref
  47.4 0.1 shard_map.88.after_ref.slot_ref
  47.5 5.5 %all-to-all-done.1.remote_ref = bf16[8,48,128]{2,1,0:T(8,128)(2,1)S(1)} async-done(((bf16[8,48,128]{2,1,0:T(8,128)(2,1)}), bf16[8,48,128]{2,1,0:T(8,128)(2,1)S(1)}, u32[]{:S(2)}, u32[]{:S(2)}) %all-to-all-start.1) | async-done | bytes 98336 | tf_op jit(solution)/shard_map/all_to_all | solution.py:371
  53.0 3.6 %shard_map.89 = bf16[8,192,128]{2,1,0:T(8,128)(2,1)S(1)} custom-call(f32[8,512]{1,0:T(8,128)S(1)} %shard_map.88.after_ref.slot_ref, f32[1,512]{1,0:T(1,128)S(1)} %broadcast_in_dim.54.bias_ref, bf16[8,16,128]{2,1,0:T(8,128)(2,1)S(1)} %get-tuple-element.22.own_ref, bf16[8,48,128]{2,1,0:T(8,128)(2,1)S(1)} %all-to-all-done.1.remote_ref, ...), custom_call_target="tpu_custom_call" | custom-call | tf_op jit(solution)/shard_map/pallas_call | solution.py:45
  56.6 11.3 %all_to_all.25.grad_ref.grads_ref = bf16[8,192,128]{2,1,0:T(8,128)(2,1)S(1)} all-to-all(bf16[8,192,128]{2,1,0:T(8,128)(2,1)S(1)} %shard_map.89), channel_id=1, replica_groups=mesh['z'=16,'y'=4,'x'=4,'core'=2] {'x','core'}, dimensions={0} | all-to-all | bytes 786432 | tf_op jit(solution)/shard_map/all_to_all | solution.py:371
  67.9 2.9 %shard_map.90 = (bf16[4,16,40,128]{3,2,1,0:T(8,128)(2,1)S(1)}, bf16[896,128]{1,0:T(8,128)(2,1)}) custom-call(f32[1,512]{1,0:T(1,128)S(1)} %convert_element_type.6.target_ref, bf16[8,192,128]{2,1,0:T(8,128)(2,1)S(1)} %all_to_all.25.grad_ref.grads_ref, bf16[896,2048]{1,0:T(8,128)(2,1)} %in_hbm.1), custom_call_target="tpu_custom_call" | custom-call | tf_op jit(solution)/shard_map/pallas_call | solution.py:45
  70.8 13.4 %all_to_all.26.in_ref = bf16[4,16,40,128]{3,2,1,0:T(8,128)(2,1)S(1)} all-to-all(bf16[4,16,40,128]{3,2,1,0:T(8,128)(2,1)S(1)} %get-tuple-element.26), channel_id=1, replica_groups=mesh['z'=16,'y'=4,'x'=4,'core'=2] {'y'}, dimensions={0} | all-to-all | bytes 1310720 | tf_op jit(solution)/shard_map/all_to_all | solution.py:371
  84.3 27.9 %all_to_all.27.returned_ref = bf16[16,64,128]{2,1,0:T(8,128)(2,1)S(1)} all-to-all(bf16[16,64,128]{2,1,0:T(8,128)(2,1)S(1)} %shard_map.91), channel_id=1, replica_groups=mesh['z'=16,'y'=4,'x'=4,'core'=2] {'z'}, dimensions={0} | all-to-all | bytes 524288 | tf_op jit(solution)/shard_map/all_to_all | solution.py:371
  112.1 0.8 shard_map.92
  (17 shorter events, 0.5 us)
Async XLA Ops:
  3.7 35.1 %all-to-all-start = ((bf16[64,8,128]{2,1,0:T(8,128)(2,1)}), bf16[64,8,128]{2,1,0:T(8,128)(2,1)S(1)}, u32[]{:S(2)}, u32[]{:S(2)}) async-start(bf16[64,8,128]{2,1,0:T(8,128)(2,1)} %bitcast.7), calls=%async_computation | async-start | bytes 262144 | tf_op jit(solution)/shard_map/all_to_all | solution.py:371
  22.1 17.7 %collective-permute-start = (bf16[2,272,128]{2,1,0:T(8,128)(2,1)}, bf16[2,272,128]{2,1,0:T(8,128)(2,1)S(1)}, u32[]{:S(2)}, u32[]{:S(2)}) collective-permute-start(bf16[2,272,128]{2,1,0:T(8,128)(2,1)} %get-tuple-element.18), channel_id=1, source_target_pairs={{0,2},{2,4},{4,6},{6,0},{1,3},{3,5},{5,7},{7,1},{8,10},{10,12},{12... | collective-permute-start | bytes 417800 | tf_op jit(solution)/shard_map/ppermute | solution.py:408
  25.5 14.3 %collective-permute-start.1 = (bf16[2,272,128]{2,1,0:T(8,128)(2,1)}, bf16[2,272,128]{2,1,0:T(8,128)(2,1)S(1)}, u32[]{:S(2)}, u32[]{:S(2)}) collective-permute-start(bf16[2,272,128]{2,1,0:T(8,128)(2,1)} %get-tuple-element.19), channel_id=1, source_target_pairs={{0,4},{2,6},{4,0},{6,2},{1,5},{3,7},{5,1},{7,3},{8,12},{10,14},{12... | collective-permute-start | bytes 417800 | tf_op jit(solution)/shard_map/ppermute | solution.py:408
  30.2 9.7 %collective-permute-start.2 = (bf16[2,272,128]{2,1,0:T(8,128)(2,1)}, bf16[2,272,128]{2,1,0:T(8,128)(2,1)S(1)}, u32[]{:S(2)}, u32[]{:S(2)}) collective-permute-start(bf16[2,272,128]{2,1,0:T(8,128)(2,1)} %get-tuple-element.20), channel_id=1, source_target_pairs={{0,6},{2,0},{4,2},{6,4},{1,7},{3,1},{5,3},{7,5},{8,14},{10,8},{12,... | collective-permute-start | bytes 417800 | tf_op jit(solution)/shard_map/ppermute | solution.py:408
  39.9 0.9 copy-start
  40.8 12.2 %collective-permute-start.3 = (bf16[4,272,128]{2,1,0:T(8,128)(2,1)S(1)}, bf16[4,272,128]{2,1,0:T(8,128)(2,1)S(1)}, u32[]{:S(2)}, u32[]{:S(2)}) collective-permute-start(bf16[4,272,128]{2,1,0:T(8,128)(2,1)S(1)} %get-tuple-element.24), channel_id=1, source_target_pairs={{0,1},{1,0},{2,3},{3,2},{4,5},{5,4},{6,7},{7,6},{8,9},{9,8},{10,11... | collective-permute-start | bytes 835592 | tf_op jit(solution)/shard_map/ppermute | solution.py:442
  42.8 10.2 %all-to-all-start.1 = ((bf16[8,48,128]{2,1,0:T(8,128)(2,1)}), bf16[8,48,128]{2,1,0:T(8,128)(2,1)S(1)}, u32[]{:S(2)}, u32[]{:S(2)}) async-start(bf16[8,48,128]{2,1,0:T(8,128)(2,1)} %shard_map.86.after_ref), calls=%async_computation.1 | async-start | bytes 196608 | tf_op jit(solution)/shard_map/all_to_all | solution.py:371

commit v6 on v5

--- a/solution.py
+++ b/solution.py
@@ -31,7 +31,7 @@
 SLOT_ROWS = CAP * PIECE
 TAIL_AT = 2 * SEND
 W_ROWS = 32
-NEAR, FAR = 4, 16
+NEAR, FAR = 8, 8
 LOG2E = 1.4426950408889634
 
 VMEM = pl.BlockSpec(memory_space=pltpu.VMEM)
@@ -53,7 +53,7 @@
 
 
 def kv_index():
-    return lax.axis_index("z") * NEAR + lax.axis_index("y")
+    return lax.axis_index("far") * NEAR + lax.axis_index("low") * 4 + lax.axis_index("y")
 
 
 def member_index():
@@ -175,6 +175,10 @@
         out_ref[t] = rows[t * ROWS : t * ROWS + REM_ROWS]
 
 
+def hold_kernel(near_hbm, out_ref):
+    out_ref[...] = near_hbm[...]
+
+
 def mate_kernel(after_ref, near_ref, one_ref, two_ref, three_ref, out_ref, kept_ref, own_ref, pair_ref):
     out_ref[0] = near_ref[SEND:TAIL_AT]
     for k, ref in enumerate((one_ref, two_ref, three_ref)):
@@ -314,9 +318,9 @@
                 continue
             term = term.T.astype(jnp.bfloat16)
             for half in range(2):
-                for d in range(NEAR):
-                    at = half * 128 + d * W_ROWS
-                    out_ref[d, 2 * i + half, :W_ROWS] = term[at : at + W_ROWS]
+                for y in range(4):
+                    at = half * 128 + y * W_ROWS
+                    out_ref[half * 4 + y, i, :W_ROWS] = term[at : at + W_ROWS]
         begin = end
     for copy in leaving:
         copy.wait()
@@ -372,7 +376,7 @@
 
 
 def body(queries, keyvals, log_sums, out_grad, inputs, selection):
-    kv_axes, tp_axes = ("z", "y"), ("x", "core")
+    kv_axes, tp_axes = ("far", "low", "y"), ("x", "core")
     me = kv_index()
     member = member_index()
     bf16 = jnp.bfloat16
@@ -403,6 +407,7 @@
         grant=ALL_VMEM,
     )
     fetched = swap(offer.reshape(KV, SLOT_ROWS, 2 * DH), kv_axes)
+    nearest = call(hold_kernel, jax.ShapeDtypeStruct(nearest.shape, bf16), [nearest])
 
     def shift(array, k):
         return lax.ppermute(array, "x", [(i, (i + k) % 4) for i in range(4)])
@@ -462,9 +467,9 @@
     )
     grads = swap(grads, tp_axes)
     near, query_grad = weight_term(target, grads, inputs)
-    near = swap(near, "y")
+    near = swap(near, ("low", "y"))
     far = call(regroup_kernel, jax.ShapeDtypeStruct((FAR, W_ROWS + NEAR * SLOT_ROWS, 2 * DH), bf16), [near])
-    far = swap(far, "z")
+    far = swap(far, "far")
     keyval_grad, weight_grad = call(
         home_kernel,
         [
@@ -477,8 +482,8 @@
 
 
 def solution(mesh):
-    split = Mesh(mesh.devices.reshape(FAR, NEAR, 4, 2), ("z", "y", "x", "core"))
-    kv, tp = ("z", "y"), ("x", "core")
+    split = Mesh(mesh.devices.reshape(FAR, 2, 4, 4, 2), ("far", "low", "y", "x", "core"))
+    kv, tp = ("far", "low", "y"), ("x", "core")
     return jax.shard_map(
         body,
         mesh=split,

time: 113 us -> 112 us (level)
  the two profiles are of different devices: /device:TPU:32 before, /device:TPU:8 now
where the time goes in v6:
time: 112 us; the launch traced here: 111 us
  blocking collectives  51.7 us (46%)
  starting transfers between devices  36.4 us (32%)
  Pallas kernels  11.6 us (10%)
  waiting for transfers between devices  8.2 us (7%)
  local copies, waits for them, and re-layouts  2.27 us (2%)
    all_to_all x3, blocking collectives, swap(): return lax.all_to_all(array, axis, 0, 0, tiled=True)  51.7 us
    all_to_all x2, starting transfers between devices, swap(): return lax.all_to_all(array, axis, 0, 0, tiled=True)  23.1 us
    pallas_call x9, Pallas kernels, call(): pl.pallas_call(kernel, out_shape=out_shape, in_specs=specs or [VMEM for _...  11.6 us
    ppermute x3, starting transfers between devices, shift(): return lax.ppermute(array, 'x', [(i, (i + k) % 4) for i in range(4)])  11.4 us
    all_to_all x2, waiting for transfers between devices, swap(): return lax.all_to_all(array, axis, 0, 0, tiled=True)  8.19 us
  transfers between devices with their start and end apart: 6, of which 2 were waited for; matrix products, arithmetic and copies ran while one was open for 2% of the time, Pallas kernels for 1%

profile of v6, /device:TPU:8, one launch (start us, length us, event | category | flops | bytes accessed | tf_op | source)
XLA Modules:
  0.0 111.4 jit_solution(18399319678654192299)
XLA Ops:
  0.6 3.1 %shard_map.85 = (bf16[512,128]{1,0:T(8,128)(2,1)}, bf16[800,128]{1,0:T(8,128)(2,1)}, bf16[2,272,128]{2,1,0:T(8,128)(2,1)}, bf16[2,272,128]{2,1,0:T(8,128)(2,1)}, bf16[2,272,128]{2,1,0:T(8,128)(2,1)}) custom-call(s32[16,448]{1,0:T(8,128)} %bitcast.8, bf16[896,128]{1,0:T(8,128)(2,1)} %kv_hbm.1, bf16[896,128]{1,0:T(8,128)(2,1)} %q_hbm.1, ...), custom_call_target="tpu_custom_call" | custom-call | tf_op jit(solution)/shard_map/pallas_call | solution.py:45
  3.7 18.7 %all-to-all-start = ((bf16[64,8,128]{2,1,0:T(8,128)(2,1)}), bf16[64,8,128]{2,1,0:T(8,128)(2,1)S(1)}, u32[]{:S(2)}, u32[]{:S(2)}) async-start(bf16[64,8,128]{2,1,0:T(8,128)(2,1)} %bitcast.7), calls=%async_computation | async-start | bytes 262144 | tf_op jit(solution)/shard_map/all_to_all | solution.py:375
  22.5 3.4 %collective-permute-start = (bf16[2,272,128]{2,1,0:T(8,128)(2,1)}, bf16[2,272,128]{2,1,0:T(8,128)(2,1)S(1)}, u32[]{:S(2)}, u32[]{:S(2)}) collective-permute-start(bf16[2,272,128]{2,1,0:T(8,128)(2,1)} %get-tuple-element.18), channel_id=1, source_target_pairs={{0,2},{2,4},{4,6},{6,0},{1,3},{3,5},{5,7},{7,1},{8,10},{10,12},{12... | collective-permute-start | bytes 417800 | tf_op jit(solution)/shard_map/ppermute | solution.py:413
  25.9 4.6 %collective-permute-start.1 = (bf16[2,272,128]{2,1,0:T(8,128)(2,1)}, bf16[2,272,128]{2,1,0:T(8,128)(2,1)S(1)}, u32[]{:S(2)}, u32[]{:S(2)}) collective-permute-start(bf16[2,272,128]{2,1,0:T(8,128)(2,1)} %get-tuple-element.19), channel_id=1, source_target_pairs={{0,4},{2,6},{4,0},{6,2},{1,5},{3,7},{5,1},{7,3},{8,12},{10,14},{12... | collective-permute-start | bytes 417800 | tf_op jit(solution)/shard_map/ppermute | solution.py:413
  30.5 3.3 %collective-permute-start.2 = (bf16[2,272,128]{2,1,0:T(8,128)(2,1)}, bf16[2,272,128]{2,1,0:T(8,128)(2,1)S(1)}, u32[]{:S(2)}, u32[]{:S(2)}) collective-permute-start(bf16[2,272,128]{2,1,0:T(8,128)(2,1)} %get-tuple-element.20), channel_id=1, source_target_pairs={{0,6},{2,0},{4,2},{6,4},{1,7},{3,1},{5,3},{7,5},{8,14},{10,8},{12,... | collective-permute-start | bytes 417800 | tf_op jit(solution)/shard_map/ppermute | solution.py:413
  33.9 0.8 dynamic-slice
  34.7 0.1 copy.13
  34.8 0.1 reshape.102
  34.9 0.2 select_reduce_fusion
  35.3 0.1 convert_element_type.6.target_ref
  35.4 0.9 copy-done
  36.4 2.7 %all-to-all-done = bf16[64,8,128]{2,1,0:T(8,128)(2,1)S(1)} async-done(((bf16[64,8,128]{2,1,0:T(8,128)(2,1)}), bf16[64,8,128]{2,1,0:T(8,128)(2,1)S(1)}, u32[]{:S(2)}, u32[]{:S(2)}) %all-to-all-start) | async-done | bytes 131104 | tf_op jit(solution)/shard_map/all_to_all | solution.py:375
  39.1 1.0 shard_map.86.after_ref
  40.1 1.9 %collective-permute-start.3 = (bf16[4,272,128]{2,1,0:T(8,128)(2,1)S(1)}, bf16[4,272,128]{2,1,0:T(8,128)(2,1)S(1)}, u32[]{:S(2)}, u32[]{:S(2)}) collective-permute-start(bf16[4,272,128]{2,1,0:T(8,128)(2,1)S(1)} %get-tuple-element.24), channel_id=1, source_target_pairs={{0,1},{1,0},{2,3},{3,2},{4,5},{5,4},{6,7},{7,6},{8,9},{9,8},{10,11... | collective-permute-start | bytes 835592 | tf_op jit(solution)/shard_map/ppermute | solution.py:447
  42.1 4.4 %all-to-all-start.1 = ((bf16[8,48,128]{2,1,0:T(8,128)(2,1)}), bf16[8,48,128]{2,1,0:T(8,128)(2,1)S(1)}, u32[]{:S(2)}, u32[]{:S(2)}) async-start(bf16[8,48,128]{2,1,0:T(8,128)(2,1)} %shard_map.86.after_ref), calls=%async_computation.1 | async-start | bytes 196608 | tf_op jit(solution)/shard_map/all_to_all | solution.py:375
  46.6 0.1 broadcast_in_dim.54.bias_ref
  46.7 0.1 shard_map.89.after_ref.slot_ref
  46.8 5.5 %all-to-all-done.1.remote_ref = bf16[8,48,128]{2,1,0:T(8,128)(2,1)S(1)} async-done(((bf16[8,48,128]{2,1,0:T(8,128)(2,1)}), bf16[8,48,128]{2,1,0:T(8,128)(2,1)S(1)}, u32[]{:S(2)}, u32[]{:S(2)}) %all-to-all-start.1) | async-done | bytes 98336 | tf_op jit(solution)/shard_map/all_to_all | solution.py:375
  52.3 3.6 %shard_map.90 = bf16[8,192,128]{2,1,0:T(8,128)(2,1)S(1)} custom-call(f32[8,512]{1,0:T(8,128)S(1)} %shard_map.89.after_ref.slot_ref, f32[1,512]{1,0:T(1,128)S(1)} %broadcast_in_dim.54.bias_ref, bf16[8,16,128]{2,1,0:T(8,128)(2,1)S(1)} %get-tuple-element.22.own_ref, bf16[8,48,128]{2,1,0:T(8,128)(2,1)S(1)} %all-to-all-done.1.remote_ref, ...), custom_call_target="tpu_custom_call" | custom-call | tf_op jit(solution)/shard_map/pallas_call | solution.py:45
  55.9 11.3 %all_to_all.25.grad_ref.grads_ref = bf16[8,192,128]{2,1,0:T(8,128)(2,1)S(1)} all-to-all(bf16[8,192,128]{2,1,0:T(8,128)(2,1)S(1)} %shard_map.90), channel_id=1, replica_groups=mesh['far'=8,'low'=2,'y'=4,'x'=4,'core'=2] {'x','core'}, dimensions={0} | all-to-all | bytes 786432 | tf_op jit(solution)/shard_map/all_to_all | solution.py:375
  67.2 2.9 %shard_map.91 = (bf16[8,8,40,128]{3,2,1,0:T(8,128)(2,1)S(1)}, bf16[896,128]{1,0:T(8,128)(2,1)}) custom-call(f32[1,512]{1,0:T(1,128)S(1)} %convert_element_type.6.target_ref, bf16[8,192,128]{2,1,0:T(8,128)(2,1)S(1)} %all_to_all.25.grad_ref.grads_ref, bf16[896,2048]{1,0:T(8,128)(2,1)} %in_hbm.1), custom_call_target="tpu_custom_call" | custom-call | tf_op jit(solution)/shard_map/pallas_call | solution.py:45
  70.1 14.1 %all_to_all.26.in_ref = bf16[8,8,40,128]{3,2,1,0:T(8,128)(2,1)S(1)} all-to-all(bf16[8,8,40,128]{3,2,1,0:T(8,128)(2,1)S(1)} %get-tuple-element.26), channel_id=1, replica_groups=mesh['far'=8,'low'=2,'y'=4,'x'=4,'core'=2] {'low','y'}, dimensions={0} | all-to-all | bytes 1310720 | tf_op jit(solution)/shard_map/all_to_all | solution.py:375
  84.2 26.3 %all_to_all.27.returned_ref = bf16[8,96,128]{2,1,0:T(8,128)(2,1)S(1)} all-to-all(bf16[8,96,128]{2,1,0:T(8,128)(2,1)S(1)} %shard_map.92), channel_id=1, replica_groups=mesh['far'=8,'low'=2,'y'=4,'x'=4,'core'=2] {'far'}, dimensions={0} | all-to-all | bytes 393216 | tf_op jit(solution)/shard_map/all_to_all | solution.py:375
  110.6 0.8 shard_map.93
  (18 shorter events, 0.5 us)
Async XLA Ops:
  3.7 35.3 %all-to-all-start = ((bf16[64,8,128]{2,1,0:T(8,128)(2,1)}), bf16[64,8,128]{2,1,0:T(8,128)(2,1)S(1)}, u32[]{:S(2)}, u32[]{:S(2)}) async-start(bf16[64,8,128]{2,1,0:T(8,128)(2,1)} %bitcast.7), calls=%async_computation | async-start | bytes 262144 | tf_op jit(solution)/shard_map/all_to_all | solution.py:375
  22.5 17.6 %collective-permute-start = (bf16[2,272,128]{2,1,0:T(8,128)(2,1)}, bf16[2,272,128]{2,1,0:T(8,128)(2,1)S(1)}, u32[]{:S(2)}, u32[]{:S(2)}) collective-permute-start(bf16[2,272,128]{2,1,0:T(8,128)(2,1)} %get-tuple-element.18), channel_id=1, source_target_pairs={{0,2},{2,4},{4,6},{6,0},{1,3},{3,5},{5,7},{7,1},{8,10},{10,12},{12... | collective-permute-start | bytes 417800 | tf_op jit(solution)/shard_map/ppermute | solution.py:413
  25.9 14.2 %collective-permute-start.1 = (bf16[2,272,128]{2,1,0:T(8,128)(2,1)}, bf16[2,272,128]{2,1,0:T(8,128)(2,1)S(1)}, u32[]{:S(2)}, u32[]{:S(2)}) collective-permute-start(bf16[2,272,128]{2,1,0:T(8,128)(2,1)} %get-tuple-element.19), channel_id=1, source_target_pairs={{0,4},{2,6},{4,0},{6,2},{1,5},{3,7},{5,1},{7,3},{8,12},{10,14},{12... | collective-permute-start | bytes 417800 | tf_op jit(solution)/shard_map/ppermute | solution.py:413
  30.5 9.5 %collective-permute-start.2 = (bf16[2,272,128]{2,1,0:T(8,128)(2,1)}, bf16[2,272,128]{2,1,0:T(8,128)(2,1)S(1)}, u32[]{:S(2)}, u32[]{:S(2)}) collective-permute-start(bf16[2,272,128]{2,1,0:T(8,128)(2,1)} %get-tuple-element.20), channel_id=1, source_target_pairs={{0,6},{2,0},{4,2},{6,4},{1,7},{3,1},{5,3},{7,5},{8,14},{10,8},{12,... | collective-permute-start | bytes 417800 | tf_op jit(solution)/shard_map/ppermute | solution.py:413
  35.4 0.9 copy-start
  40.1 12.2 %collective-permute-start.3 = (bf16[4,272,128]{2,1,0:T(8,128)(2,1)S(1)}, bf16[4,272,128]{2,1,0:T(8,128)(2,1)S(1)}, u32[]{:S(2)}, u32[]{:S(2)}) collective-permute-start(bf16[4,272,128]{2,1,0:T(8,128)(2,1)S(1)} %get-tuple-element.24), channel_id=1, source_target_pairs={{0,1},{1,0},{2,3},{3,2},{4,5},{5,4},{6,7},{7,6},{8,9},{9,8},{10,11... | collective-permute-start | bytes 835592 | tf_op jit(solution)/shard_map/ppermute | solution.py:447
  42.1 10.2 %all-to-all-start.1 = ((bf16[8,48,128]{2,1,0:T(8,128)(2,1)}), bf16[8,48,128]{2,1,0:T(8,128)(2,1)S(1)}, u32[]{:S(2)}, u32[]{:S(2)}) async-start(bf16[8,48,128]{2,1,0:T(8,128)(2,1)} %shard_map.86.after_ref), calls=%async_computation.1 | async-start | bytes 196608 | tf_op jit(solution)/shard_map/all_to_all | solution.py:375

commit v7 on v6

--- a/solution.py
+++ b/solution.py
@@ -30,6 +30,7 @@
 SEND = LOG_AT + 16
 SLOT_ROWS = CAP * PIECE
 TAIL_AT = 2 * SEND
+TAIL = 2 * QB + 2 * NSEL
 W_ROWS = 32
 NEAR, FAR = 8, 8
 LOG2E = 1.4426950408889634
@@ -100,6 +101,14 @@
     mine = mine.astype(jnp.bfloat16)
     gets[0].wait()
     local = (sel_ref[...] - me * OWN).astype(jnp.float32)
+    chosen = sel_ref[...].astype(jnp.float32)
+    owner = jnp.floor((chosen + 0.5) * (1.0 / OWN))
+    lists = (KV * PER, 128)
+    ours = lax.broadcasted_iota(jnp.int32, lists, 0) - me * PER == lax.broadcasted_iota(jnp.int32, lists, 1)
+    ours = (ours & (lax.broadcasted_iota(jnp.int32, lists, 1) < PER)).astype(jnp.bfloat16)
+    for i, part in enumerate((owner, chosen - owner * OWN)):
+        part = jnp.dot(part.astype(jnp.bfloat16), ours, preferred_element_type=jnp.float32)
+        tail_ref[2 * QB + i * NSEL : 2 * QB + (i + 1) * NSEL] = part.astype(jnp.bfloat16)
     inside = (local >= 0) & (local < OWN)
     least = jnp.min(jnp.where(inside, local, 1000.0), axis=0, keepdims=True)
     most = jnp.max(jnp.where(inside, local, -1000.0), axis=0, keepdims=True)
@@ -141,8 +150,8 @@
     own_at = pl.multiple_of(jnp.minimum(member, PER - 1) * QB, QB)
     own = jnp.dot(turn, kv_ref[pl.ds(own_at, QB)], preferred_element_type=jnp.float32)
     tail_ref[:QB] = own.astype(jnp.bfloat16)
-    tail_ref[QB:] = pair_ref[...].astype(jnp.bfloat16)
-    copies.append(pltpu.make_async_copy(tail_ref, near_hbm.at[pl.ds(TAIL_AT, 2 * QB)], sems.at[5]))
+    tail_ref[QB : 2 * QB] = pair_ref[...].astype(jnp.bfloat16)
+    copies.append(pltpu.make_async_copy(tail_ref, near_hbm.at[pl.ds(TAIL_AT, TAIL)], sems.at[5]))
     copies[-1].start()
     piece = jnp.dot(mine, kv_ref[...], preferred_element_type=jnp.float32).astype(jnp.bfloat16)
     at = lax.broadcasted_iota(jnp.int32, (SLOT_ROWS, 128), 1) - (
@@ -175,8 +184,12 @@
         out_ref[t] = rows[t * ROWS : t * ROWS + REM_ROWS]
 
 
-def hold_kernel(near_hbm, out_ref):
-    out_ref[...] = near_hbm[...]
+def hold_kernel(near_ref, out_ref, list_ref):
+    out_ref[...] = near_ref[...]
+    at = TAIL_AT + 2 * QB
+    owner = near_ref[at : at + NSEL].astype(jnp.float32)
+    within = near_ref[at + NSEL : at + 2 * NSEL].astype(jnp.float32)
+    list_ref[...] = (owner * OWN + within).astype(jnp.int32)
 
 
 def mate_kernel(after_ref, near_ref, one_ref, two_ref, three_ref, out_ref, kept_ref, own_ref, pair_ref):
@@ -185,7 +198,7 @@
         out_ref[k + 1] = ref[1]
     kept_ref[...] = near_ref[:SEND]
     own_ref[...] = near_ref[TAIL_AT : TAIL_AT + QB].reshape(TP, DIAG * PIECE, 2 * DH)
-    pair_ref[...] = near_ref[TAIL_AT + QB :]
+    pair_ref[...] = near_ref[TAIL_AT + QB : TAIL_AT + 2 * QB]
 
 
 def attention_kernel(
@@ -377,7 +390,6 @@
 
 def body(queries, keyvals, log_sums, out_grad, inputs, selection):
     kv_axes, tp_axes = ("far", "low", "y"), ("x", "core")
-    me = kv_index()
     member = member_index()
     bf16 = jnp.bfloat16
 
@@ -386,7 +398,7 @@
         offer_kernel,
         [
             jax.ShapeDtypeStruct((SLOTS, 2 * DH), bf16),
-            jax.ShapeDtypeStruct((TAIL_AT + 2 * QB, 2 * DH), bf16),
+            jax.ShapeDtypeStruct((TAIL_AT + TAIL, 2 * DH), bf16),
             *[block] * 3,
         ],
         [selection.T, keyvals, queries, out_grad, log_sums],
@@ -398,7 +410,7 @@
             pltpu.VMEM((2, TOK), jnp.float32),
             pltpu.VMEM((16, TOK), bf16),
             pltpu.VMEM((2 * KV, 128), jnp.float32),
-            pltpu.VMEM((2 * QB, 2 * DH), bf16),
+            pltpu.VMEM((TAIL, 2 * DH), bf16),
             pltpu.SemaphoreType.DMA((6,)),
             pltpu.SemaphoreType.DMA((TP, 3)),
         ],
@@ -407,14 +419,18 @@
         grant=ALL_VMEM,
     )
     fetched = swap(offer.reshape(KV, SLOT_ROWS, 2 * DH), kv_axes)
-    nearest = call(hold_kernel, jax.ShapeDtypeStruct(nearest.shape, bf16), [nearest])
+    nearest, lists = call(
+        hold_kernel,
+        [jax.ShapeDtypeStruct(nearest.shape, bf16), jax.ShapeDtypeStruct((NSEL, 128), jnp.int32)],
+        [nearest],
+    )
 
     def shift(array, k):
         return lax.ppermute(array, "x", [(i, (i + k) % 4) for i in range(4)])
 
     two, one, three = shift(blocks[1], 2), shift(blocks[0], 1), shift(blocks[2], 3)
 
-    mine = lax.dynamic_slice(selection, (me * PER, 0), (PER, NSEL))[:, DIAG:]
+    mine = lists[DIAG:, :PER].T
     flat = mine.reshape(-1)
     owner = flat // OWN
     alike = owner[:, None] == owner[None, :]

time: 112 us -> 112 us (level)
  no operation moved by 1% of the time
where the time goes in v7:
time: 112 us
  blocking collectives  51.7 us (46%)
  starting transfers between devices  36.4 us (32%)
  Pallas kernels  11.6 us (10%)
  waiting for transfers between devices  8.01 us (7%)
  local copies, waits for them, and re-layouts  2.26 us (2%)
  other arithmetic  1.15 us (1%)
    all_to_all x3, blocking collectives, swap(): return lax.all_to_all(array, axis, 0, 0, tiled=True)  51.7 us
    all_to_all x2, starting transfers between devices, swap(): return lax.all_to_all(array, axis, 0, 0, tiled=True)  23.1 us
    pallas_call x9, Pallas kernels, call(): pl.pallas_call(kernel, out_shape=out_shape, in_specs=specs or [VMEM for _...  11.6 us
    ppermute x3, starting transfers between devices, shift(): return lax.ppermute(array, 'x', [(i, (i + k) % 4) for i in range(4)])  11.4 us
    all_to_all x2, waiting for transfers between devices, swap(): return lax.all_to_all(array, axis, 0, 0, tiled=True)  8 us
  transfers between devices with their start and end apart: 6, of which 2 were waited for; matrix products, arithmetic and copies ran while one was open for 2% of the time, Pallas kernels for 1%

profile of v7, /device:TPU:8, one launch (start us, length us, event | category | flops | bytes accessed | tf_op | source)
XLA Modules:
  0.0 111.9 jit_solution(14457029592066898322)
XLA Ops:
  0.6 3.1 %shard_map.85 = (bf16[512,128]{1,0:T(8,128)(2,1)}, bf16[832,128]{1,0:T(8,128)(2,1)}, bf16[2,272,128]{2,1,0:T(8,128)(2,1)}, bf16[2,272,128]{2,1,0:T(8,128)(2,1)}, bf16[2,272,128]{2,1,0:T(8,128)(2,1)}) custom-call(s32[16,448]{1,0:T(8,128)} %bitcast.10, bf16[896,128]{1,0:T(8,128)(2,1)} %kv_hbm.1, bf16[896,128]{1,0:T(8,128)(2,1)} %q_hbm.1, ...), custom_call_target="tpu_custom_call" | custom-call | tf_op jit(solution)/shard_map/pallas_call | solution.py:46
  3.7 18.7 %all-to-all-start = ((bf16[64,8,128]{2,1,0:T(8,128)(2,1)}), bf16[64,8,128]{2,1,0:T(8,128)(2,1)S(1)}, u32[]{:S(2)}, u32[]{:S(2)}) async-start(bf16[64,8,128]{2,1,0:T(8,128)(2,1)} %bitcast.9), calls=%async_computation | async-start | bytes 262144 | tf_op jit(solution)/shard_map/all_to_all | solution.py:388
  22.5 3.4 %collective-permute-start = (bf16[2,272,128]{2,1,0:T(8,128)(2,1)}, bf16[2,272,128]{2,1,0:T(8,128)(2,1)S(1)}, u32[]{:S(2)}, u32[]{:S(2)}) collective-permute-start(bf16[2,272,128]{2,1,0:T(8,128)(2,1)} %get-tuple-element.22), channel_id=1, source_target_pairs={{0,2},{2,4},{4,6},{6,0},{1,3},{3,5},{5,7},{7,1},{8,10},{10,12},{12... | collective-permute-start | bytes 417800 | tf_op jit(solution)/shard_map/ppermute | solution.py:429
  25.9 4.6 %collective-permute-start.1 = (bf16[2,272,128]{2,1,0:T(8,128)(2,1)}, bf16[2,272,128]{2,1,0:T(8,128)(2,1)S(1)}, u32[]{:S(2)}, u32[]{:S(2)}) collective-permute-start(bf16[2,272,128]{2,1,0:T(8,128)(2,1)} %get-tuple-element.23), channel_id=1, source_target_pairs={{0,4},{2,6},{4,0},{6,2},{1,5},{3,7},{5,1},{7,3},{8,12},{10,14},{12... | collective-permute-start | bytes 417800 | tf_op jit(solution)/shard_map/ppermute | solution.py:429
  30.5 3.3 %collective-permute-start.2 = (bf16[2,272,128]{2,1,0:T(8,128)(2,1)}, bf16[2,272,128]{2,1,0:T(8,128)(2,1)S(1)}, u32[]{:S(2)}, u32[]{:S(2)}) collective-permute-start(bf16[2,272,128]{2,1,0:T(8,128)(2,1)} %get-tuple-element.24), channel_id=1, source_target_pairs={{0,6},{2,0},{4,2},{6,4},{1,7},{3,1},{5,3},{7,5},{8,14},{10,8},{12,... | collective-permute-start | bytes 417800 | tf_op jit(solution)/shard_map/ppermute | solution.py:429
  33.9 0.9 copy-done
  35.0 0.2 select_reduce_fusion
  35.3 0.1 copy.16
  35.6 0.1 convert_element_type.6.target_ref
  35.7 3.3 %all-to-all-done = bf16[64,8,128]{2,1,0:T(8,128)(2,1)S(1)} async-done(((bf16[64,8,128]{2,1,0:T(8,128)(2,1)}), bf16[64,8,128]{2,1,0:T(8,128)(2,1)S(1)}, u32[]{:S(2)}, u32[]{:S(2)}) %all-to-all-start) | async-done | bytes 131104 | tf_op jit(solution)/shard_map/all_to_all | solution.py:388
  39.0 1.0 shard_map.87.after_ref
  40.1 1.9 %collective-permute-start.3 = (bf16[4,272,128]{2,1,0:T(8,128)(2,1)S(1)}, bf16[4,272,128]{2,1,0:T(8,128)(2,1)S(1)}, u32[]{:S(2)}, u32[]{:S(2)}) collective-permute-start(bf16[4,272,128]{2,1,0:T(8,128)(2,1)S(1)} %get-tuple-element.28), channel_id=1, source_target_pairs={{0,1},{1,0},{2,3},{3,2},{4,5},{5,4},{6,7},{7,6},{8,9},{9,8},{10,11... | collective-permute-start | bytes 835592 | tf_op jit(solution)/shard_map/ppermute | solution.py:463
  42.0 0.6 dynamic-slice
  42.6 4.4 %all-to-all-start.1 = ((bf16[8,48,128]{2,1,0:T(8,128)(2,1)}), bf16[8,48,128]{2,1,0:T(8,128)(2,1)S(1)}, u32[]{:S(2)}, u32[]{:S(2)}) async-start(bf16[8,48,128]{2,1,0:T(8,128)(2,1)} %shard_map.87.after_ref), calls=%async_computation.1 | async-start | bytes 196608 | tf_op jit(solution)/shard_map/all_to_all | solution.py:388
  47.0 0.8 select_reduce_fusion.1
  47.9 0.1 broadcast_in_dim.54.bias_ref
  48.0 0.1 shard_map.89.after_ref.slot_ref
  48.2 4.7 %all-to-all-done.1.remote_ref = bf16[8,48,128]{2,1,0:T(8,128)(2,1)S(1)} async-done(((bf16[8,48,128]{2,1,0:T(8,128)(2,1)}), bf16[8,48,128]{2,1,0:T(8,128)(2,1)S(1)}, u32[]{:S(2)}, u32[]{:S(2)}) %all-to-all-start.1) | async-done | bytes 98336 | tf_op jit(solution)/shard_map/all_to_all | solution.py:388
  52.8 3.6 %shard_map.90 = bf16[8,192,128]{2,1,0:T(8,128)(2,1)S(1)} custom-call(f32[8,512]{1,0:T(8,128)S(1)} %shard_map.89.after_ref.slot_ref, f32[1,512]{1,0:T(1,128)S(1)} %broadcast_in_dim.54.bias_ref, bf16[8,16,128]{2,1,0:T(8,128)(2,1)S(1)} %get-tuple-element.26.own_ref, bf16[8,48,128]{2,1,0:T(8,128)(2,1)S(1)} %all-to-all-done.1.remote_ref, ...), custom_call_target="tpu_custom_call" | custom-call | tf_op jit(solution)/shard_map/pallas_call | solution.py:46
  56.4 11.3 %all_to_all.25.grad_ref.grads_ref = bf16[8,192,128]{2,1,0:T(8,128)(2,1)S(1)} all-to-all(bf16[8,192,128]{2,1,0:T(8,128)(2,1)S(1)} %shard_map.90), channel_id=1, replica_groups=mesh['far'=8,'low'=2,'y'=4,'x'=4,'core'=2] {'x','core'}, dimensions={0} | all-to-all | bytes 786432 | tf_op jit(solution)/shard_map/all_to_all | solution.py:388
  67.7 2.9 %shard_map.91 = (bf16[8,8,40,128]{3,2,1,0:T(8,128)(2,1)S(1)}, bf16[896,128]{1,0:T(8,128)(2,1)}) custom-call(f32[1,512]{1,0:T(1,128)S(1)} %convert_element_type.6.target_ref, bf16[8,192,128]{2,1,0:T(8,128)(2,1)S(1)} %all_to_all.25.grad_ref.grads_ref, bf16[896,2048]{1,0:T(8,128)(2,1)} %in_hbm.1), custom_call_target="tpu_custom_call" | custom-call | tf_op jit(solution)/shard_map/pallas_call | solution.py:46
  70.6 14.1 %all_to_all.26.in_ref = bf16[8,8,40,128]{3,2,1,0:T(8,128)(2,1)S(1)} all-to-all(bf16[8,8,40,128]{3,2,1,0:T(8,128)(2,1)S(1)} %get-tuple-element.30), channel_id=1, replica_groups=mesh['far'=8,'low'=2,'y'=4,'x'=4,'core'=2] {'low','y'}, dimensions={0} | all-to-all | bytes 1310720 | tf_op jit(solution)/shard_map/all_to_all | solution.py:388
  84.8 26.3 %all_to_all.27.returned_ref = bf16[8,96,128]{2,1,0:T(8,128)(2,1)S(1)} all-to-all(bf16[8,96,128]{2,1,0:T(8,128)(2,1)S(1)} %shard_map.92), channel_id=1, replica_groups=mesh['far'=8,'low'=2,'y'=4,'x'=4,'core'=2] {'far'}, dimensions={0} | all-to-all | bytes 393216 | tf_op jit(solution)/shard_map/all_to_all | solution.py:388
  111.1 0.8 shard_map.93
  (20 shorter events, 0.7 us)
Async XLA Ops:
  3.7 35.3 %all-to-all-start = ((bf16[64,8,128]{2,1,0:T(8,128)(2,1)}), bf16[64,8,128]{2,1,0:T(8,128)(2,1)S(1)}, u32[]{:S(2)}, u32[]{:S(2)}) async-start(bf16[64,8,128]{2,1,0:T(8,128)(2,1)} %bitcast.9), calls=%async_computation | async-start | bytes 262144 | tf_op jit(solution)/shard_map/all_to_all | solution.py:388
  22.5 17.6 %collective-permute-start = (bf16[2,272,128]{2,1,0:T(8,128)(2,1)}, bf16[2,272,128]{2,1,0:T(8,128)(2,1)S(1)}, u32[]{:S(2)}, u32[]{:S(2)}) collective-permute-start(bf16[2,272,128]{2,1,0:T(8,128)(2,1)} %get-tuple-element.22), channel_id=1, source_target_pairs={{0,2},{2,4},{4,6},{6,0},{1,3},{3,5},{5,7},{7,1},{8,10},{10,12},{12... | collective-permute-start | bytes 417800 | tf_op jit(solution)/shard_map/ppermute | solution.py:429
  25.9 14.2 %collective-permute-start.1 = (bf16[2,272,128]{2,1,0:T(8,128)(2,1)}, bf16[2,272,128]{2,1,0:T(8,128)(2,1)S(1)}, u32[]{:S(2)}, u32[]{:S(2)}) collective-permute-start(bf16[2,272,128]{2,1,0:T(8,128)(2,1)} %get-tuple-element.23), channel_id=1, source_target_pairs={{0,4},{2,6},{4,0},{6,2},{1,5},{3,7},{5,1},{7,3},{8,12},{10,14},{12... | collective-permute-start | bytes 417800 | tf_op jit(solution)/shard_map/ppermute | solution.py:429
  30.5 9.5 %collective-permute-start.2 = (bf16[2,272,128]{2,1,0:T(8,128)(2,1)}, bf16[2,272,128]{2,1,0:T(8,128)(2,1)S(1)}, u32[]{:S(2)}, u32[]{:S(2)}) collective-permute-start(bf16[2,272,128]{2,1,0:T(8,128)(2,1)} %get-tuple-element.24), channel_id=1, source_target_pairs={{0,6},{2,0},{4,2},{6,4},{1,7},{3,1},{5,3},{7,5},{8,14},{10,8},{12,... | collective-permute-start | bytes 417800 | tf_op jit(solution)/shard_map/ppermute | solution.py:429
  33.9 0.9 copy-start
  40.1 12.7 %collective-permute-start.3 = (bf16[4,272,128]{2,1,0:T(8,128)(2,1)S(1)}, bf16[4,272,128]{2,1,0:T(8,128)(2,1)S(1)}, u32[]{:S(2)}, u32[]{:S(2)}) collective-permute-start(bf16[4,272,128]{2,1,0:T(8,128)(2,1)S(1)} %get-tuple-element.28), channel_id=1, source_target_pairs={{0,1},{1,0},{2,3},{3,2},{4,5},{5,4},{6,7},{7,6},{8,9},{9,8},{10,11... | collective-permute-start | bytes 835592 | tf_op jit(solution)/shard_map/ppermute | solution.py:463
  42.6 10.2 %all-to-all-start.1 = ((bf16[8,48,128]{2,1,0:T(8,128)(2,1)}), bf16[8,48,128]{2,1,0:T(8,128)(2,1)S(1)}, u32[]{:S(2)}, u32[]{:S(2)}) async-start(bf16[8,48,128]{2,1,0:T(8,128)(2,1)} %shard_map.87.after_ref), calls=%async_computation.1 | async-start | bytes 196608 | tf_op jit(solution)/shard_map/all_to_all | solution.py:388
